TPU v7x, 512 devices: a 4x2x32 block of a 4x8x32 slice. The times are simulated.
512 devices in a mesh: grp: 2 (over y), fs: 32 (over z), tp: 8 (over x, core).
Axes of the slice: x: 4, y: 2, z: 32, core: 2. Of those that a mesh axis runs over, the one named last changes fastest.
The devices are a block of a 4x8x32 slice.
Arguments:
- tokens: bfloat16 [16384, 2048], P(('grp', 'fs')), parts along dimension 0, may hold values from -6 to 6
- norm_gain: float32 [2048], P('fs'), may hold values from 0.1 to 1.9
- gate_master: float32 [32, 2048, 1024], P(None, 'fs', 'tp'), may hold values from -0.125 to 0.125
- up_master: float32 [32, 2048, 1024], P(None, 'fs', 'tp'), may hold values from -0.125 to 0.125
- chosen: int32 [16384, 2], P(('grp', 'fs')), parts along dimension 0, may hold values from 0 to 31, all different within a row; in each aligned block of 256 rows (0 to 255, 256 to 511, ...) at most 32 rows name the same one
- affinity: float32 [16384, 2], P(('grp', 'fs')), parts along dimension 0, may hold values from 0.05 to 1
Outputs:
- gate_served: bfloat16 [64, 2048, 1024], P(('grp', 'fs'), None, 'tp'), parts along dimension 0
- up_served: bfloat16 [64, 2048, 1024], P(('grp', 'fs'), None, 'tp'), parts along dimension 0
- hidden: bfloat16 [16384, 2, 1024], P(('grp', 'fs'), None, 'tp'), parts along dimension 0
There are 2 independent parts, one for each index of `grp`. A program takes and returns all parts, laid end to end along the dimension named above; an argument that names none is the same for every part. Nothing has to cross between parts.
Inputs may be any that keep to these rules, and one draw needn't show every extreme that they name: Among the rows of one index of fs (256 tokens, all their choices) no expert is chosen more than 32 times, a bound that some block reaches; the choices of one token differ.
All inputs are finite; a program needn't handle non-finite values.
Results may differ from a plain program's by a relative error of at most 0.023.
Values may be sent and summed in bfloat16 or wider, within the bound.
No kernel may reach another device: no remote copies, remote signals or barrier semaphores. Data moves between devices by JAX's collectives and lax.ppermute only.
A program may use at most 64 MiB of HBM per device.

v0:
```python
import functools
import jax
import jax.numpy as jnp
from jax import lax
from jax.experimental import pallas as pl
from jax.experimental.pallas import tpu as pltpu
from jax.sharding import PartitionSpec as P

F32 = jnp.float32
BF16 = jnp.bfloat16
CORES = 2
TILE = 8
STEPS = 4


def iota(shape, dim):
    return lax.broadcasted_iota(jnp.int32, shape, dim)


def dot(a, b, dims=(((1,), (0,)), ((), ()))):
    return lax.dot_general(a, b, dims, preferred_element_type=F32)


def column(row):
    n = row.shape[1]
    return jnp.sum(jnp.where(iota((n, n), 0) == iota((n, n), 1), row, 0.0), axis=1, keepdims=True)


def slots_of(choice, experts):
    top, n = choice.shape
    expert = iota((experts, n), 0).astype(F32)
    named = jnp.zeros((experts, n), F32)
    for k in range(top):
        named = named + (choice[k : k + 1, :] == expert).astype(F32)
    before = (iota((n, n), 0) < iota((n, n), 1)).astype(F32).astype(BF16)
    return named, dot(named.astype(BF16), before)


def pack_kernel(tokens, chosen, gain, gate, up, out, gains, *, experts, capacity, narrow, piece):
    n, width = tokens.shape
    x = tokens[...].astype(F32)
    scale = lax.rsqrt(jnp.sum(x * x, axis=-1, keepdims=True) / width + 1e-06)
    at = pl.multiple_of(lax.axis_index("tp") * narrow, narrow)
    own = (tokens[:, pl.ds(at, narrow)].astype(F32) * scale).astype(BF16)
    named, slot = slots_of(chosen[...].astype(F32), experts)
    slot = jnp.where(named > 0, slot, -1.0)
    pick = slot[:, None, :] == iota((experts, capacity, n), 1).astype(F32)
    pick = pick.astype(F32).reshape(experts * capacity, n).astype(BF16)
    out[:, :capacity, :] = dot(pick, own).astype(BF16).reshape(experts, capacity, narrow)
    half = gate.shape[2]
    gains[...] = jnp.broadcast_to(column(gain[...]), gains.shape)
    at = pl.multiple_of(lax.axis_index("grp") * piece, TILE)
    g = gains[pl.ds(at, piece), :][None]
    out[:, capacity:, :half] = (gate[:, pl.ds(at, piece), :] * g).astype(BF16)
    out[:, capacity:, half:] = (up[:, pl.ds(at, piece), :] * g).astype(BF16)


def expert_kernel(*refs, parts, cores):
    gate, up, hidden, mixed = refs[-4:]
    weights, slices = refs[:parts], refs[parts:-4]
    half = gate.shape[2]
    total = len(slices)
    narrow = slices[0].shape[1]

    @pl.when(pl.program_id(0) == 0)
    def _():
        piece = weights[0].shape[2]
        mine = lax.axis_index("grp")
        q = 0
        for ref in weights:
            for j in range(ref.shape[0]):
                at = pl.multiple_of((mine ^ q) * piece, TILE)
                gate[:, pl.ds(at, piece), :] = ref[j, :, :, :half]
                up[:, pl.ds(at, piece), :] = ref[j, :, :, half:]
                q += 1
        tp = lax.axis_index("tp")
        per = gate.shape[0] // total
        for k, where in enumerate(slice_places(total, cores)):
            at = where(tp) * per
            mixed[k, :, :half] = gate[pl.ds(at, per)].reshape(narrow, half)
            mixed[k, :, half:] = up[pl.ds(at, per)].reshape(narrow, half)

    a = dot(slices[0][...], mixed[0])
    for k in range(1, total):
        a = a + dot(slices[k][...], mixed[k])
    g = a[:, :half]
    hidden[...] = (g / (1.0 + jnp.exp(-g)) * a[:, half:]).astype(BF16)


def place_kernel(chosen, affinity, take, share, *, experts, capacity):
    top, n = chosen.shape
    lines, total = take.shape
    choice = chosen[...].astype(F32)
    _, slot = slots_of(choice, experts)
    expert = iota((experts, n), 0).astype(F32)
    a = affinity[...]
    part = a / jnp.sum(a, axis=0, keepdims=True)
    line = iota((lines, n), 0)
    here = line // top == iota((lines, n), 1)
    at = jnp.zeros((lines, n), F32)
    of = jnp.zeros((lines, n), F32)
    for k in range(top):
        c = choice[k : k + 1, :]
        goal = jnp.sum(jnp.where(c == expert, slot, 0.0), axis=0, keepdims=True) + c * capacity
        this = here & (line % top == k)
        at = jnp.where(this, goal, at)
        of = jnp.where(this, part[k : k + 1, :], of)
    at = jnp.sum(at, axis=1, keepdims=True)
    take[...] = (iota((lines, total), 1).astype(F32) == at).astype(F32).astype(BF16)
    share[...] = jnp.broadcast_to(jnp.sum(of, axis=1, keepdims=True), share.shape)


def pick_kernel(back, take, share, out):
    out[...] = (dot(take[...], back[...]) * share[...]).astype(BF16)


def ring_tables(total, cores):
    def hop(sign):
        def to(i):
            turn = sign if i % cores == 0 else -sign
            return (i + turn * cores) % total

        return [(i, to(i)) for i in range(total)]

    return hop(1), hop(-1), [(i, i ^ 1) for i in range(total)]


def slice_places(total, cores):
    chips = total // cores

    def away(steps):
        def place(i):
            turn = jnp.where(i % cores == 0, -steps, steps)
            return (i + turn * cores + total) % total

        return place

    places = [away(0)]
    for s in range(1, chips // 2 + 1):
        places.append(away(s))
        if s <= (chips - 1) // 2:
            places.append(away(-s))
    return places + [lambda i, p=p: p(i ^ 1) for p in places]


def gather_slices(own, total, cores):
    ahead, behind, swap = ring_tables(total, cores)
    chips = total // cores
    got = [own]
    one = two = own
    for s in range(1, chips // 2 + 1):
        one = lax.ppermute(one, "tp", ahead)
        got.append(one)
        if s <= (chips - 1) // 2:
            two = lax.ppermute(two, "tp", behind)
            got.append(two)
    return got + [lax.ppermute(g, "tp", swap) for g in got]


def gather_groups(own, groups):
    got = [own]
    step = 1
    while step < groups:
        send = got[0] if len(got) == 1 else jnp.concatenate(got, axis=0)
        table = [(i, i ^ step) for i in range(groups)]
        got.append(lax.ppermute(send, "grp", table))
        step *= 2
    return got


def on_device(tokens, norm_gain, gate_master, up_master, chosen, affinity):
    groups, sources, total = (lax.axis_size(a) for a in ("grp", "fs", "tp"))
    experts, block, half = gate_master.shape
    n, width = tokens.shape
    top = chosen.shape[1]
    capacity = n * top * 2 // experts
    narrow = width // total
    piece = block // groups
    vmem = pl.BlockSpec(memory_space=pltpu.VMEM)

    sent = pl.pallas_call(
        functools.partial(
            pack_kernel, experts=experts, capacity=capacity, narrow=narrow, piece=piece
        ),
        out_shape=jax.ShapeDtypeStruct((experts, capacity + piece, narrow), BF16),
        in_specs=[vmem] * 5,
        out_specs=vmem,
        scratch_shapes=[pltpu.VMEM((block, half), F32)],
        name="pack",
    )(tokens, chosen.T, norm_gain[None, :], gate_master, up_master)
    got = lax.all_to_all(sent, "fs", split_axis=0, concat_axis=0, tiled=True)
    rows = got[:, :capacity, :].reshape(sources * capacity, narrow)
    weights = gather_groups(got[None, :, capacity:, :], groups)
    slices = gather_slices(rows, total, CORES)

    slots = sources * capacity
    rows_at = lambda i: (i, 0)
    fixed = lambda dims: pl.BlockSpec(dims, lambda i: (0,) * len(dims))
    gate, up, hidden = pl.pallas_call(
        functools.partial(expert_kernel, parts=len(weights), cores=CORES),
        grid=(STEPS,),
        out_shape=(
            jax.ShapeDtypeStruct((sources, block, half), BF16),
            jax.ShapeDtypeStruct((sources, block, half), BF16),
            jax.ShapeDtypeStruct((slots, half), BF16),
        ),
        in_specs=[fixed(w.shape) for w in weights]
        + [pl.BlockSpec((slots // STEPS, narrow), rows_at) for _ in slices],
        out_specs=(
            fixed((sources, block, half)),
            fixed((sources, block, half)),
            pl.BlockSpec((slots // STEPS, half), rows_at),
        ),
        scratch_shapes=[pltpu.VMEM((total, narrow, 2 * half), BF16)],
        name="experts",
    )(*weights, *slices)
    hidden, choice, ratio = lax.optimization_barrier((hidden, chosen.T, affinity.T))
    back = lax.all_to_all(
        hidden.reshape(sources, capacity, half), "fs", split_axis=0, concat_axis=0, tiled=True
    )
    take, share = pl.pallas_call(
        functools.partial(place_kernel, experts=experts, capacity=capacity),
        out_shape=(
            jax.ShapeDtypeStruct((n * top, experts * capacity), BF16),
            jax.ShapeDtypeStruct((n * top, half), F32),
        ),
        in_specs=[vmem] * 2,
        out_specs=(vmem, vmem),
        name="place",
    )(choice, ratio)
    out = pl.pallas_call(
        pick_kernel,
        out_shape=jax.ShapeDtypeStruct((n * top, half), BF16),
        in_specs=[vmem] * 3,
        out_specs=vmem,
        name="pick",
    )(back.reshape(experts * capacity, half), take, share)
    return (
        gate.reshape(1, sources * block, half),
        up.reshape(1, sources * block, half),
        out.reshape(n, top, half),
    )


def solution(mesh):
    return jax.shard_map(
        on_device,
        mesh=mesh,
        in_specs=(
            P(("grp", "fs"), None),
            P("fs"),
            P(None, "fs", "tp"),
            P(None, "fs", "tp"),
            P(("grp", "fs"), None),
            P(("grp", "fs"), None),
        ),
        out_specs=(
            P(("grp", "fs"), None, "tp"),
            P(("grp", "fs"), None, "tp"),
            P(("grp", "fs"), None, "tp"),
        ),
        check_vma=False,
    )
```

profile of v0, /device:TPU:34, one launch (start us, length us, event | category | flops | bytes accessed | tf_op | source)
XLA Modules:
  0.0 253.7 jit_solution(6961345178637040547)
XLA Ops:
  0.6 3.5 %pack.1 = bf16[32,64,256]{2,1,0:T(8,128)(2,1)} custom-call(bf16[256,2048]{1,0:T(8,128)(2,1)} %tokens.1, s32[2,256]{1,0:T(2,128)} %bitcast.18, f32[1,64]{1,0:T(1,128)} %bitcast.21, f32[32,64,128]{2,1,0:T(8,128)} %gate.1, f32[32,64,128]{2,1,0:T(8,128)} %up.1), custom_call_target="tpu_custom_call" | custom-call | tf_op jit(solution)/shard_map/pack/pallas_call | solution.py:181
  4.2 150.3 %all_to_all.10 = bf16[32,64,256]{2,1,0:T(8,128)(2,1)S(1)} all-to-all(bf16[32,64,256]{2,1,0:T(8,128)(2,1)} %pack.1), channel_id=1, replica_groups=mesh['grp'=2,'fs'=32,'tp'=8] {'fs'}, dimensions={0} | all-to-all | bytes 2097152 | tf_op jit(solution)/shard_map/all_to_all | solution.py:191
  154.4 0.1 fusion
  154.5 3.6 %collective-permute-start.1 = (bf16[1024,256]{1,0:T(8,128)(2,1)S(1)}, bf16[1024,256]{1,0:T(8,128)(2,1)S(1)}, u32[]{:S(2)}, u32[]{:S(2)}) collective-permute-start(bf16[1024,256]{1,0:T(8,128)(2,1)S(1)} %bitcast.11), channel_id=1, source_target_pairs={{0,2},{1,7},{2,4},{3,1},{4,6},{5,3},{6,0},{7,5},{8,10},{9,15},{10,... | collective-permute-start | bytes 1572872 | tf_op jit(solution)/shard_map/ppermute | solution.py:152
  158.1 2.3 collective-permute-start.2
  160.4 9.3 %collective-permute-done.1.refs_3_ = bf16[1024,256]{1,0:T(8,128)(2,1)S(1)} collective-permute-done((bf16[1024,256]{1,0:T(8,128)(2,1)S(1)}, bf16[1024,256]{1,0:T(8,128)(2,1)S(1)}, u32[]{:S(2)}, u32[]{:S(2)}) %collective-permute-start.1) | collective-permute-done | bytes 524320 | tf_op jit(solution)/shard_map/ppermute | solution.py:152
  169.7 4.4 %collective-permute-start.3 = (bf16[1024,256]{1,0:T(8,128)(2,1)S(1)}, bf16[1024,256]{1,0:T(8,128)(2,1)S(1)}, u32[]{:S(2)}, u32[]{:S(2)}) collective-permute-start(bf16[1024,256]{1,0:T(8,128)(2,1)S(1)} %collective-permute-done.1.refs_3_), channel_id=1, source_target_pairs={{0,2},{1,7},{2,4},{3,1},{4,6},{5,3},{6,0},{7,5},{8,10},{9,15},{10,... | collective-permute-start | bytes 1572872 | tf_op jit(solution)/shard_map/ppermute | solution.py:152
  174.1 2.0 collective-permute-start.4
  176.1 4.0 %collective-permute-start = (bf16[1,32,32,256]{3,2,1,0:T(8,128)(2,1)S(1)}, bf16[1,32,32,256]{3,2,1,0:T(8,128)(2,1)S(1)}, u32[]{:S(2)}, u32[]{:S(2)}) collective-permute-start(bf16[1,32,32,256]{3,2,1,0:T(8,128)(2,1)S(1)} %get-tuple-element.20.refs_0_), channel_id=1, source_target_pairs={{0,256},{256,0},{1,257},{257,1},{2,258},{258,2},{3,259},{259,3},{4... | collective-permute-start | bytes 1572872 | tf_op jit(solution)/shard_map/ppermute | solution.py:166
  180.1 2.2 collective-permute-start.5
  182.3 0.0 collective-permute-done.2.refs_4_
  182.3 2.2 collective-permute-start.6
  184.6 0.0 collective-permute-done.3.refs_5_
  184.6 2.2 collective-permute-start.7
  186.7 0.0 collective-permute-done.4.refs_6_
  186.8 5.9 %collective-permute-done.refs_1_ = bf16[1,32,32,256]{3,2,1,0:T(8,128)(2,1)S(1)} collective-permute-done((bf16[1,32,32,256]{3,2,1,0:T(8,128)(2,1)S(1)}, bf16[1,32,32,256]{3,2,1,0:T(8,128)(2,1)S(1)}, u32[]{:S(2)}, u32[]{:S(2)}) %collective-permute-start) | collective-permute-done | bytes 524320 | tf_op jit(solution)/shard_map/ppermute | solution.py:166
  192.7 0.0 collective-permute-done.6.refs_8_
  192.7 0.0 collective-permute-done.5.refs_7_
  192.7 0.8 copy-done.7
  193.5 0.2 copy-done.9
  193.7 0.8 copy-done.8
  194.5 0.0 collective-permute-done.7.refs_9_
  194.5 0.0 copy-done.3
  194.5 0.0 copy-done.4
  194.5 0.0 copy-done.5
  194.5 0.0 copy-done.6
  194.5 5.7 %experts.1 = (bf16[32,64,128]{2,1,0:T(8,128)(2,1)}, bf16[32,64,128]{2,1,0:T(8,128)(2,1)}, bf16[1024,128]{1,0:T(8,128)(2,1)}) custom-call(bf16[1,32,32,256]{3,2,1,0:T(8,128)(2,1)} %copy-done.1, bf16[1,32,32,256]{3,2,1,0:T(8,128)(2,1)} %copy-done.7, bf16[1024,256]{1,0:T(8,128)(2,1)} %bitcast.14, bf16[1024,256]{1,0:T(8,128)(2,1)} %copy-done.3, ...), custom_call_target="tpu_custom_call" | custom-call | tf_op jit(solution)/shard_map/experts/pallas_call | solution.py:199
  200.2 8.4 %all-to-all-start.1 = ((bf16[32,32,128]{2,1,0:T(8,128)(2,1)}), bf16[32,32,128]{2,1,0:T(8,128)(2,1)S(1)}, u32[]{:S(2)}, u32[]{:S(2)}) async-start(bf16[32,32,128]{2,1,0:T(8,128)(2,1)} %bitcast.16), calls=%async_computation.1 | async-start | bytes 524288 | tf_op jit(solution)/shard_map/all_to_all | solution.py:218
  208.7 2.1 place.1
  210.8 39.8 %all-to-all-done.1 = bf16[32,32,128]{2,1,0:T(8,128)(2,1)S(1)} async-done(((bf16[32,32,128]{2,1,0:T(8,128)(2,1)}), bf16[32,32,128]{2,1,0:T(8,128)(2,1)S(1)}, u32[]{:S(2)}, u32[]{:S(2)}) %all-to-all-start.1) | async-done | bytes 262176 | tf_op jit(solution)/shard_map/all_to_all | solution.py:218
  250.6 0.7 copy-done.2
  251.3 2.4 pick.1
  (12 shorter events, 0.0 us)
Async XLA Ops:
  154.5 40.0 %copy-start = (bf16[32,32,256]{2,1,0:T(8,128)(2,1)}, bf16[32,32,256]{2,1,0:T(8,128)(2,1)S(1)}, u32[]{:S(2)}) copy-start(bf16[32,32,256]{2,1,0:T(8,128)(2,1)S(1)} %get-tuple-element.19) | copy-start | bytes 1572868
  154.5 40.0 %copy-start.1 = (bf16[1,32,32,256]{3,2,1,0:T(8,128)(2,1)}, bf16[1,32,32,256]{3,2,1,0:T(8,128)(2,1)S(1)}, u32[]{:S(2)}) copy-start(bf16[1,32,32,256]{3,2,1,0:T(8,128)(2,1)S(1)} %get-tuple-element.20.refs_0_) | copy-start | bytes 1572868
  154.5 15.2 %collective-permute-start.1 = (bf16[1024,256]{1,0:T(8,128)(2,1)S(1)}, bf16[1024,256]{1,0:T(8,128)(2,1)S(1)}, u32[]{:S(2)}, u32[]{:S(2)}) collective-permute-start(bf16[1024,256]{1,0:T(8,128)(2,1)S(1)} %bitcast.11), channel_id=1, source_target_pairs={{0,2},{1,7},{2,4},{3,1},{4,6},{5,3},{6,0},{7,5},{8,10},{9,15},{10,... | collective-permute-start | bytes 1572872 | tf_op jit(solution)/shard_map/ppermute | solution.py:152
  158.1 24.2 %collective-permute-start.2 = (bf16[1024,256]{1,0:T(8,128)(2,1)S(1)}, bf16[1024,256]{1,0:T(8,128)(2,1)S(1)}, u32[]{:S(2)}, u32[]{:S(2)}) collective-permute-start(bf16[1024,256]{1,0:T(8,128)(2,1)S(1)} %bitcast.12), channel_id=1, source_target_pairs={{0,6},{1,3},{2,0},{3,5},{4,2},{5,7},{6,4},{7,1},{8,14},{9,11},{10,... | collective-permute-start | bytes 1572872 | tf_op jit(solution)/shard_map/ppermute | solution.py:155
  169.7 24.8 %copy-start.3 = (bf16[1024,256]{1,0:T(8,128)(2,1)}, bf16[1024,256]{1,0:T(8,128)(2,1)S(1)}, u32[]{:S(2)}) copy-start(bf16[1024,256]{1,0:T(8,128)(2,1)S(1)} %collective-permute-done.1.refs_3_) | copy-start | bytes 1572868
  169.7 14.8 %collective-permute-start.3 = (bf16[1024,256]{1,0:T(8,128)(2,1)S(1)}, bf16[1024,256]{1,0:T(8,128)(2,1)S(1)}, u32[]{:S(2)}, u32[]{:S(2)}) collective-permute-start(bf16[1024,256]{1,0:T(8,128)(2,1)S(1)} %collective-permute-done.1.refs_3_), channel_id=1, source_target_pairs={{0,2},{1,7},{2,4},{3,1},{4,6},{5,3},{6,0},{7,5},{8,10},{9,15},{10,... | collective-permute-start | bytes 1572872 | tf_op jit(solution)/shard_map/ppermute | solution.py:152
  174.1 12.6 %collective-permute-start.4 = (bf16[1024,256]{1,0:T(8,128)(2,1)S(1)}, bf16[1024,256]{1,0:T(8,128)(2,1)S(1)}, u32[]{:S(2)}, u32[]{:S(2)}) collective-permute-start(bf16[1024,256]{1,0:T(8,128)(2,1)S(1)} %bitcast.13), channel_id=1, source_target_pairs={{0,1},{1,0},{2,3},{3,2},{4,5},{5,4},{6,7},{7,6},{8,9},{9,8},{10,11... | collective-permute-start | bytes 1572872 | tf_op jit(solution)/shard_map/ppermute | solution.py:157
  176.1 16.6 %collective-permute-start = (bf16[1,32,32,256]{3,2,1,0:T(8,128)(2,1)S(1)}, bf16[1,32,32,256]{3,2,1,0:T(8,128)(2,1)S(1)}, u32[]{:S(2)}, u32[]{:S(2)}) collective-permute-start(bf16[1,32,32,256]{3,2,1,0:T(8,128)(2,1)S(1)} %get-tuple-element.20.refs_0_), channel_id=1, source_target_pairs={{0,256},{256,0},{1,257},{257,1},{2,258},{258,2},{3,259},{259,3},{4... | collective-permute-start | bytes 1572872 | tf_op jit(solution)/shard_map/ppermute | solution.py:166
  180.1 12.6 %collective-permute-start.5 = (bf16[1024,256]{1,0:T(8,128)(2,1)S(1)}, bf16[1024,256]{1,0:T(8,128)(2,1)S(1)}, u32[]{:S(2)}, u32[]{:S(2)}) collective-permute-start(bf16[1024,256]{1,0:T(8,128)(2,1)S(1)} %collective-permute-done.1.refs_3_), channel_id=1, source_target_pairs={{0,1},{1,0},{2,3},{3,2},{4,5},{5,4},{6,7},{7,6},{8,9},{9,8},{10,11... | collective-permute-start | bytes 1572872 | tf_op jit(solution)/shard_map/ppermute | solution.py:157
  182.3 12.2 %copy-start.4 = (bf16[1024,256]{1,0:T(8,128)(2,1)}, bf16[1024,256]{1,0:T(8,128)(2,1)S(1)}, u32[]{:S(2)}) copy-start(bf16[1024,256]{1,0:T(8,128)(2,1)S(1)} %collective-permute-done.2.refs_4_) | copy-start | bytes 1572868
  182.3 10.4 %collective-permute-start.6 = (bf16[1024,256]{1,0:T(8,128)(2,1)S(1)}, bf16[1024,256]{1,0:T(8,128)(2,1)S(1)}, u32[]{:S(2)}, u32[]{:S(2)}) collective-permute-start(bf16[1024,256]{1,0:T(8,128)(2,1)S(1)} %collective-permute-done.2.refs_4_), channel_id=1, source_target_pairs={{0,1},{1,0},{2,3},{3,2},{4,5},{5,4},{6,7},{7,6},{8,9},{9,8},{10,11... | collective-permute-start | bytes 1572872 | tf_op jit(solution)/shard_map/ppermute | solution.py:157
  184.6 9.9 %copy-start.5 = (bf16[1024,256]{1,0:T(8,128)(2,1)}, bf16[1024,256]{1,0:T(8,128)(2,1)S(1)}, u32[]{:S(2)}) copy-start(bf16[1024,256]{1,0:T(8,128)(2,1)S(1)} %collective-permute-done.3.refs_5_) | copy-start | bytes 1572868
  184.6 9.9 %collective-permute-start.7 = (bf16[1024,256]{1,0:T(8,128)(2,1)S(1)}, bf16[1024,256]{1,0:T(8,128)(2,1)}, u32[]{:S(2)}, u32[]{:S(2)}) collective-permute-start(bf16[1024,256]{1,0:T(8,128)(2,1)S(1)} %collective-permute-done.3.refs_5_), channel_id=1, source_target_pairs={{0,1},{1,0},{2,3},{3,2},{4,5},{5,4},{6,7},{7,6},{8,9},{9,8},{10,11... | collective-permute-start | bytes 1572872 | tf_op jit(solution)/shard_map/ppermute | solution.py:157
  186.7 7.8 %copy-start.6 = (bf16[1024,256]{1,0:T(8,128)(2,1)}, bf16[1024,256]{1,0:T(8,128)(2,1)S(1)}, u32[]{:S(2)}) copy-start(bf16[1024,256]{1,0:T(8,128)(2,1)S(1)} %collective-permute-done.4.refs_6_) | copy-start | bytes 1572868
  192.7 0.8 copy-start.7
  192.7 1.0 copy-start.9
  193.7 0.8 copy-start.8
  200.2 50.4 %all-to-all-start.1 = ((bf16[32,32,128]{2,1,0:T(8,128)(2,1)}), bf16[32,32,128]{2,1,0:T(8,128)(2,1)S(1)}, u32[]{:S(2)}, u32[]{:S(2)}) async-start(bf16[32,32,128]{2,1,0:T(8,128)(2,1)} %bitcast.16), calls=%async_computation.1 | async-start | bytes 524288 | tf_op jit(solution)/shard_map/all_to_all | solution.py:218
  250.6 0.7 copy-start.2
where the time goes:
time: 254 us
  blocking collectives  150 us (59%)
  waiting for transfers between devices  55 us (22%)
  starting transfers between devices  31.3 us (12%)
  Pallas kernels  13.8 us (5%)
  local copies, waits for them, and re-layouts  2.56 us (1%)
    all_to_all x1, blocking collectives, on_device(): got = lax.all_to_all(sent, 'fs', split_axis=0, concat_axis=0, tiled=True)  150 us
    all_to_all x1, waiting for transfers between devices, on_device(): lax.all_to_all(hidden.reshape(sources, capacity, half), 'fs', split_axis=...  39.8 us
    ppermute x2, waiting for transfers between devices, gather_slices(): one = lax.ppermute(one, 'tp', ahead)  9.28 us
    ppermute x4, starting transfers between devices, gather_slices(): return got + [lax.ppermute(g, 'tp', swap) for g in got]  8.5 us
    all_to_all x1, starting transfers between devices, on_device(): lax.all_to_all(hidden.reshape(sources, capacity, half), 'fs', split_axis=...  8.43 us
    ppermute x2, starting transfers between devices, gather_slices(): one = lax.ppermute(one, 'tp', ahead)  7.97 us
    ppermute x1, waiting for transfers between devices, gather_groups(): got.append(lax.ppermute(send, 'grp', table))  5.94 us
    pallas_call x1, Pallas kernels, on_device(): pl.pallas_call(functools.partial(expert_kernel, parts=len(weights), cores...  5.72 us
  transfers between devices with their start and end apart: 9, of which 3 were waited for; matrix products, arithmetic and copies ran while one was open for 0% of the time, Pallas kernels for 1%

commit v1 on v0

--- a/solution.py
+++ b/solution.py
@@ -10,7 +10,7 @@
 BF16 = jnp.bfloat16
 CORES = 2
 TILE = 8
-STEPS = 4
+PARAMS = pltpu.CompilerParams(vmem_limit_bytes=16 << 20)
 
 
 def iota(shape, dim):
@@ -62,24 +62,21 @@
     total = len(slices)
     narrow = slices[0].shape[1]
 
-    @pl.when(pl.program_id(0) == 0)
-    def _():
-        piece = weights[0].shape[2]
-        mine = lax.axis_index("grp")
-        q = 0
-        for ref in weights:
-            for j in range(ref.shape[0]):
-                at = pl.multiple_of((mine ^ q) * piece, TILE)
-                gate[:, pl.ds(at, piece), :] = ref[j, :, :, :half]
-                up[:, pl.ds(at, piece), :] = ref[j, :, :, half:]
-                q += 1
-        tp = lax.axis_index("tp")
-        per = gate.shape[0] // total
-        for k, where in enumerate(slice_places(total, cores)):
-            at = where(tp) * per
-            mixed[k, :, :half] = gate[pl.ds(at, per)].reshape(narrow, half)
-            mixed[k, :, half:] = up[pl.ds(at, per)].reshape(narrow, half)
-
+    piece = weights[0].shape[2]
+    mine = lax.axis_index("grp")
+    q = 0
+    for ref in weights:
+        for j in range(ref.shape[0]):
+            at = pl.multiple_of((mine ^ q) * piece, TILE)
+            gate[:, pl.ds(at, piece), :] = ref[j, :, :, :half]
+            up[:, pl.ds(at, piece), :] = ref[j, :, :, half:]
+            q += 1
+    tp = lax.axis_index("tp")
+    per = gate.shape[0] // total
+    for k, where in enumerate(slice_places(total, cores)):
+        at = where(tp) * per
+        mixed[k, :, :half] = gate[pl.ds(at, per)].reshape(narrow, half)
+        mixed[k, :, half:] = up[pl.ds(at, per)].reshape(narrow, half)
     a = dot(slices[0][...], mixed[0])
     for k in range(1, total):
         a = a + dot(slices[k][...], mixed[k])
@@ -186,6 +183,7 @@
         in_specs=[vmem] * 5,
         out_specs=vmem,
         scratch_shapes=[pltpu.VMEM((block, half), F32)],
+        compiler_params=PARAMS,
         name="pack",
     )(tokens, chosen.T, norm_gain[None, :], gate_master, up_master)
     got = lax.all_to_all(sent, "fs", split_axis=0, concat_axis=0, tiled=True)
@@ -193,25 +191,17 @@
     weights = gather_groups(got[None, :, capacity:, :], groups)
     slices = gather_slices(rows, total, CORES)
 
-    slots = sources * capacity
-    rows_at = lambda i: (i, 0)
-    fixed = lambda dims: pl.BlockSpec(dims, lambda i: (0,) * len(dims))
     gate, up, hidden = pl.pallas_call(
         functools.partial(expert_kernel, parts=len(weights), cores=CORES),
-        grid=(STEPS,),
         out_shape=(
             jax.ShapeDtypeStruct((sources, block, half), BF16),
             jax.ShapeDtypeStruct((sources, block, half), BF16),
-            jax.ShapeDtypeStruct((slots, half), BF16),
-        ),
-        in_specs=[fixed(w.shape) for w in weights]
-        + [pl.BlockSpec((slots // STEPS, narrow), rows_at) for _ in slices],
-        out_specs=(
-            fixed((sources, block, half)),
-            fixed((sources, block, half)),
-            pl.BlockSpec((slots // STEPS, half), rows_at),
-        ),
+            jax.ShapeDtypeStruct((sources * capacity, half), BF16),
+        ),
+        in_specs=[vmem] * (len(weights) + len(slices)),
+        out_specs=(vmem, vmem, vmem),
         scratch_shapes=[pltpu.VMEM((total, narrow, 2 * half), BF16)],
+        compiler_params=PARAMS,
         name="experts",
     )(*weights, *slices)
     hidden, choice, ratio = lax.optimization_barrier((hidden, chosen.T, affinity.T))
@@ -226,6 +216,7 @@
         ),
         in_specs=[vmem] * 2,
         out_specs=(vmem, vmem),
+        compiler_params=PARAMS,
         name="place",
     )(choice, ratio)
     out = pl.pallas_call(
@@ -233,6 +224,7 @@
         out_shape=jax.ShapeDtypeStruct((n * top, half), BF16),
         in_specs=[vmem] * 3,
         out_specs=vmem,
+        compiler_params=PARAMS,
         name="pick",
     )(back.reshape(experts * capacity, half), take, share)
     return (

time: 254 us -> 249 us (0.980)
  Pallas kernels: 13.8 us -> 4.55 us
    pallas_call x1, Pallas kernels: 5.72 us -> 2.36 us  [on_device(): pl.pallas_call(functools.partial(expert_kernel, parts=len(weights), cores...]
    pallas_call x1, Pallas kernels: 3.54 us -> 0.67 us  [on_device(): pl.pallas_call(functools.partial(pack_kernel, experts=experts, capacity=c...]
  transfers between devices with their start and end apart: 9 -> 9, of which waited for: 3 -> 3; matrix products, arithmetic and copies ran while one was open for 0% -> 0% of each run, Pallas kernels for 1% -> 0%
where the time goes in v1:
time: 249 us; the launch traced here: 248 us
  blocking collectives  150 us (60%)
  waiting for transfers between devices  56.8 us (23%)
  starting transfers between devices  31.4 us (13%)
  Pallas kernels  4.55 us (2%)
  local copies, waits for them, and re-layouts  4.41 us (2%)
    all_to_all x1, blocking collectives, on_device(): got = lax.all_to_all(sent, 'fs', split_axis=0, concat_axis=0, tiled=True)  150 us
    all_to_all x1, waiting for transfers between devices, on_device(): lax.all_to_all(hidden.reshape(sources, capacity, half), 'fs', split_axis=...  41.5 us
    ppermute x2, waiting for transfers between devices, gather_slices(): one = lax.ppermute(one, 'tp', ahead)  9.29 us
    all_to_all x1, starting transfers between devices, on_device(): lax.all_to_all(hidden.reshape(sources, capacity, half), 'fs', split_axis=...  8.54 us
    ppermute x4, starting transfers between devices, gather_slices(): return got + [lax.ppermute(g, 'tp', swap) for g in got]  8.5 us
    ppermute x2, starting transfers between devices, gather_slices(): one = lax.ppermute(one, 'tp', ahead)  7.98 us
    ppermute x1, waiting for transfers between devices, gather_groups(): got.append(lax.ppermute(send, 'grp', table))  5.97 us
  transfers between devices with their start and end apart: 9, of which 3 were waited for; matrix products, arithmetic and copies ran while one was open for 0% of the time, Pallas kernels for 0%

profile of v1, /device:TPU:34, one launch (start us, length us, event | category | flops | bytes accessed | tf_op | source)
XLA Modules:
  0.0 248.0 jit_solution(17725624814781537871)
XLA Ops:
  0.6 0.0 copy-start.3
  0.6 0.0 copy-start.5
  0.7 0.7 copy-done.3
  1.3 0.0 copy-done.5
  1.3 1.2 copy-done
  2.5 1.2 copy-done.1
  3.8 1.2 copy-done.2
  5.0 0.7 pack.1
  5.7 150.0 %all_to_all.10 = bf16[32,64,256]{2,1,0:T(8,128)(2,1)S(1)} all-to-all(bf16[32,64,256]{2,1,0:T(8,128)(2,1)S(1)} %pack.1), channel_id=1, replica_groups=mesh['grp'=2,'fs'=32,'tp'=8] {'fs'}, dimensions={0} | all-to-all | bytes 2097152 | tf_op jit(solution)/shard_map/all_to_all | solution.py:189
  155.7 0.1 fusion
  155.8 3.6 %collective-permute-start.1 = (bf16[1024,256]{1,0:T(8,128)(2,1)S(1)}, bf16[1024,256]{1,0:T(8,128)(2,1)S(1)}, u32[]{:S(2)}, u32[]{:S(2)}) collective-permute-start(bf16[1024,256]{1,0:T(8,128)(2,1)S(1)} %bitcast.11), channel_id=1, source_target_pairs={{0,2},{1,7},{2,4},{3,1},{4,6},{5,3},{6,0},{7,5},{8,10},{9,15},{10,... | collective-permute-start | bytes 1572872 | tf_op jit(solution)/shard_map/ppermute | solution.py:149
  159.4 2.3 collective-permute-start.2
  161.7 9.3 %collective-permute-done.1.refs_3_ = bf16[1024,256]{1,0:T(8,128)(2,1)S(1)} collective-permute-done((bf16[1024,256]{1,0:T(8,128)(2,1)S(1)}, bf16[1024,256]{1,0:T(8,128)(2,1)S(1)}, u32[]{:S(2)}, u32[]{:S(2)}) %collective-permute-start.1) | collective-permute-done | bytes 524320 | tf_op jit(solution)/shard_map/ppermute | solution.py:149
  171.0 4.4 %collective-permute-start.3 = (bf16[1024,256]{1,0:T(8,128)(2,1)S(1)}, bf16[1024,256]{1,0:T(8,128)(2,1)S(1)}, u32[]{:S(2)}, u32[]{:S(2)}) collective-permute-start(bf16[1024,256]{1,0:T(8,128)(2,1)S(1)} %collective-permute-done.1.refs_3_), channel_id=1, source_target_pairs={{0,2},{1,7},{2,4},{3,1},{4,6},{5,3},{6,0},{7,5},{8,10},{9,15},{10,... | collective-permute-start | bytes 1572872 | tf_op jit(solution)/shard_map/ppermute | solution.py:149
  175.4 2.0 collective-permute-start.4
  177.4 4.1 %collective-permute-start = (bf16[1,32,32,256]{3,2,1,0:T(8,128)(2,1)S(1)}, bf16[1,32,32,256]{3,2,1,0:T(8,128)(2,1)S(1)}, u32[]{:S(2)}, u32[]{:S(2)}) collective-permute-start(bf16[1,32,32,256]{3,2,1,0:T(8,128)(2,1)S(1)} %get-tuple-element.20.refs_0_), channel_id=1, source_target_pairs={{0,256},{256,0},{1,257},{257,1},{2,258},{258,2},{3,259},{259,3},{4... | collective-permute-start | bytes 1572872 | tf_op jit(solution)/shard_map/ppermute | solution.py:163
  181.4 2.2 collective-permute-start.5
  183.6 0.0 collective-permute-done.2.refs_4_
  183.6 2.2 collective-permute-start.6
  185.9 0.0 collective-permute-done.3.refs_5_
  185.9 2.2 collective-permute-start.7
  188.0 0.0 collective-permute-done.4.refs_6_
  188.0 6.0 %collective-permute-done.refs_1_ = bf16[1,32,32,256]{3,2,1,0:T(8,128)(2,1)S(1)} collective-permute-done((bf16[1,32,32,256]{3,2,1,0:T(8,128)(2,1)S(1)}, bf16[1,32,32,256]{3,2,1,0:T(8,128)(2,1)S(1)}, u32[]{:S(2)}, u32[]{:S(2)}) %collective-permute-start) | collective-permute-done | bytes 524320 | tf_op jit(solution)/shard_map/ppermute | solution.py:163
  194.0 0.0 collective-permute-done.6.refs_8_
  194.0 0.0 collective-permute-done.5.refs_7_
  194.0 0.0 collective-permute-done.7.refs_9_
  194.0 2.4 experts.1
  196.4 8.5 %all-to-all-start.1 = ((bf16[32,32,128]{2,1,0:T(8,128)(2,1)}), bf16[32,32,128]{2,1,0:T(8,128)(2,1)S(1)}, u32[]{:S(2)}, u32[]{:S(2)}) async-start(bf16[32,32,128]{2,1,0:T(8,128)(2,1)} %bitcast.7), calls=%async_computation.1 | async-start | bytes 524288 | tf_op jit(solution)/shard_map/all_to_all | solution.py:208
  204.9 0.0 copy-done.4
  204.9 0.4 place.1
  205.4 41.5 %all-to-all-done.1 = bf16[32,32,128]{2,1,0:T(8,128)(2,1)S(1)} async-done(((bf16[32,32,128]{2,1,0:T(8,128)(2,1)}), bf16[32,32,128]{2,1,0:T(8,128)(2,1)S(1)}, u32[]{:S(2)}, u32[]{:S(2)}) %all-to-all-start.1) | async-done | bytes 262176 | tf_op jit(solution)/shard_map/all_to_all | solution.py:208
  246.9 1.1 pick.1
  (4 shorter events, 0.0 us)
Async XLA Ops:
  0.6 0.7 copy-start.3
  0.6 0.7 copy-start.5
  1.3 1.2 copy-start
  2.5 1.2 copy-start.1
  3.8 1.2 copy-start.2
  155.8 15.2 %collective-permute-start.1 = (bf16[1024,256]{1,0:T(8,128)(2,1)S(1)}, bf16[1024,256]{1,0:T(8,128)(2,1)S(1)}, u32[]{:S(2)}, u32[]{:S(2)}) collective-permute-start(bf16[1024,256]{1,0:T(8,128)(2,1)S(1)} %bitcast.11), channel_id=1, source_target_pairs={{0,2},{1,7},{2,4},{3,1},{4,6},{5,3},{6,0},{7,5},{8,10},{9,15},{10,... | collective-permute-start | bytes 1572872 | tf_op jit(solution)/shard_map/ppermute | solution.py:149
  159.4 24.2 %collective-permute-start.2 = (bf16[1024,256]{1,0:T(8,128)(2,1)S(1)}, bf16[1024,256]{1,0:T(8,128)(2,1)S(1)}, u32[]{:S(2)}, u32[]{:S(2)}) collective-permute-start(bf16[1024,256]{1,0:T(8,128)(2,1)S(1)} %bitcast.12), channel_id=1, source_target_pairs={{0,6},{1,3},{2,0},{3,5},{4,2},{5,7},{6,4},{7,1},{8,14},{9,11},{10,... | collective-permute-start | bytes 1572872 | tf_op jit(solution)/shard_map/ppermute | solution.py:152
  171.0 14.9 %collective-permute-start.3 = (bf16[1024,256]{1,0:T(8,128)(2,1)S(1)}, bf16[1024,256]{1,0:T(8,128)(2,1)S(1)}, u32[]{:S(2)}, u32[]{:S(2)}) collective-permute-start(bf16[1024,256]{1,0:T(8,128)(2,1)S(1)} %collective-permute-done.1.refs_3_), channel_id=1, source_target_pairs={{0,2},{1,7},{2,4},{3,1},{4,6},{5,3},{6,0},{7,5},{8,10},{9,15},{10,... | collective-permute-start | bytes 1572872 | tf_op jit(solution)/shard_map/ppermute | solution.py:149
  175.4 12.6 %collective-permute-start.4 = (bf16[1024,256]{1,0:T(8,128)(2,1)S(1)}, bf16[1024,256]{1,0:T(8,128)(2,1)S(1)}, u32[]{:S(2)}, u32[]{:S(2)}) collective-permute-start(bf16[1024,256]{1,0:T(8,128)(2,1)S(1)} %bitcast.13), channel_id=1, source_target_pairs={{0,1},{1,0},{2,3},{3,2},{4,5},{5,4},{6,7},{7,6},{8,9},{9,8},{10,11... | collective-permute-start | bytes 1572872 | tf_op jit(solution)/shard_map/ppermute | solution.py:154
  177.4 16.6 %collective-permute-start = (bf16[1,32,32,256]{3,2,1,0:T(8,128)(2,1)S(1)}, bf16[1,32,32,256]{3,2,1,0:T(8,128)(2,1)S(1)}, u32[]{:S(2)}, u32[]{:S(2)}) collective-permute-start(bf16[1,32,32,256]{3,2,1,0:T(8,128)(2,1)S(1)} %get-tuple-element.20.refs_0_), channel_id=1, source_target_pairs={{0,256},{256,0},{1,257},{257,1},{2,258},{258,2},{3,259},{259,3},{4... | collective-permute-start | bytes 1572872 | tf_op jit(solution)/shard_map/ppermute | solution.py:163
  181.4 12.6 %collective-permute-start.5 = (bf16[1024,256]{1,0:T(8,128)(2,1)S(1)}, bf16[1024,256]{1,0:T(8,128)(2,1)S(1)}, u32[]{:S(2)}, u32[]{:S(2)}) collective-permute-start(bf16[1024,256]{1,0:T(8,128)(2,1)S(1)} %collective-permute-done.1.refs_3_), channel_id=1, source_target_pairs={{0,1},{1,0},{2,3},{3,2},{4,5},{5,4},{6,7},{7,6},{8,9},{9,8},{10,11... | collective-permute-start | bytes 1572872 | tf_op jit(solution)/shard_map/ppermute | solution.py:154
  183.6 10.4 %collective-permute-start.6 = (bf16[1024,256]{1,0:T(8,128)(2,1)S(1)}, bf16[1024,256]{1,0:T(8,128)(2,1)S(1)}, u32[]{:S(2)}, u32[]{:S(2)}) collective-permute-start(bf16[1024,256]{1,0:T(8,128)(2,1)S(1)} %collective-permute-done.2.refs_4_), channel_id=1, source_target_pairs={{0,1},{1,0},{2,3},{3,2},{4,5},{5,4},{6,7},{7,6},{8,9},{9,8},{10,11... | collective-permute-start | bytes 1572872 | tf_op jit(solution)/shard_map/ppermute | solution.py:154
  185.9 8.2 %collective-permute-start.7 = (bf16[1024,256]{1,0:T(8,128)(2,1)S(1)}, bf16[1024,256]{1,0:T(8,128)(2,1)S(1)}, u32[]{:S(2)}, u32[]{:S(2)}) collective-permute-start(bf16[1024,256]{1,0:T(8,128)(2,1)S(1)} %collective-permute-done.3.refs_5_), channel_id=1, source_target_pairs={{0,1},{1,0},{2,3},{3,2},{4,5},{5,4},{6,7},{7,6},{8,9},{9,8},{10,11... | collective-permute-start | bytes 1572872 | tf_op jit(solution)/shard_map/ppermute | solution.py:154
  196.4 8.6 %copy-start.4 = (f32[256,2]{0,1:T(2,128)S(1)}, f32[256,2]{0,1:T(2,128)}, u32[]{:S(2)}) copy-start(f32[256,2]{0,1:T(2,128)} %param.11) | copy-start | bytes 6148
  196.4 50.5 %all-to-all-start.1 = ((bf16[32,32,128]{2,1,0:T(8,128)(2,1)}), bf16[32,32,128]{2,1,0:T(8,128)(2,1)S(1)}, u32[]{:S(2)}, u32[]{:S(2)}) async-start(bf16[32,32,128]{2,1,0:T(8,128)(2,1)} %bitcast.7), calls=%async_computation.1 | async-start | bytes 524288 | tf_op jit(solution)/shard_map/all_to_all | solution.py:208

commit v2 on v1

--- a/solution.py
+++ b/solution.py
@@ -10,6 +10,7 @@
 BF16 = jnp.bfloat16
 CORES = 2
 TILE = 8
+PARTS = 4
 PARAMS = pltpu.CompilerParams(vmem_limit_bytes=16 << 20)
 
 
@@ -36,23 +37,39 @@
     return named, dot(named.astype(BF16), before)
 
 
-def pack_kernel(tokens, chosen, gain, gate, up, out, gains, *, experts, capacity, narrow, piece):
-    n, width = tokens.shape
-    x = tokens[...].astype(F32)
-    scale = lax.rsqrt(jnp.sum(x * x, axis=-1, keepdims=True) / width + 1e-06)
-    at = pl.multiple_of(lax.axis_index("tp") * narrow, narrow)
-    own = (tokens[:, pl.ds(at, narrow)].astype(F32) * scale).astype(BF16)
-    named, slot = slots_of(chosen[...].astype(F32), experts)
+def pack_kernel(
+    tokens, chosen, gain, gate, up, out, tok, cho, gai, gat, upp, gains, sems, *, experts, capacity
+):
+    n, width = tok.shape
+    narrow = out.shape[2]
+    piece, half = gat.shape[1:]
+    part = n // PARTS
+    mine = pl.multiple_of(lax.axis_index("grp") * piece, TILE)
+    pairs = [(chosen, cho), (gain, gai)]
+    pairs += [(tokens.at[pl.ds(i * part, part)], tok.at[pl.ds(i * part, part)]) for i in range(PARTS)]
+    pairs += [(gate.at[:, pl.ds(mine, piece), :], gat), (up.at[:, pl.ds(mine, piece), :], upp)]
+    copies = [pltpu.make_async_copy(a, b, sems.at[i]) for i, (a, b) in enumerate(pairs)]
+    for c in copies:
+        c.start()
+    copies[0].wait()
+    named, slot = slots_of(cho[...].astype(F32), experts)
     slot = jnp.where(named > 0, slot, -1.0)
     pick = slot[:, None, :] == iota((experts, capacity, n), 1).astype(F32)
     pick = pick.astype(F32).reshape(experts * capacity, n).astype(BF16)
+    copies[1].wait()
+    gains[...] = jnp.broadcast_to(column(gai[...]), gains.shape)
+    for c in copies[2 : 2 + PARTS]:
+        c.wait()
+    x = tok[...].astype(F32)
+    scale = lax.rsqrt(jnp.sum(x * x, axis=-1, keepdims=True) / width + 1e-06)
+    at = pl.multiple_of(lax.axis_index("tp") * narrow, narrow)
+    own = (tok[:, pl.ds(at, narrow)].astype(F32) * scale).astype(BF16)
     out[:, :capacity, :] = dot(pick, own).astype(BF16).reshape(experts, capacity, narrow)
-    half = gate.shape[2]
-    gains[...] = jnp.broadcast_to(column(gain[...]), gains.shape)
-    at = pl.multiple_of(lax.axis_index("grp") * piece, TILE)
-    g = gains[pl.ds(at, piece), :][None]
-    out[:, capacity:, :half] = (gate[:, pl.ds(at, piece), :] * g).astype(BF16)
-    out[:, capacity:, half:] = (up[:, pl.ds(at, piece), :] * g).astype(BF16)
+    for c in copies[2 + PARTS :]:
+        c.wait()
+    g = gains[pl.ds(mine, piece), :][None]
+    out[:, capacity:, :half] = (gat[...] * g).astype(BF16)
+    out[:, capacity:, half:] = (upp[...] * g).astype(BF16)
 
 
 def expert_kernel(*refs, parts, cores):
@@ -176,16 +193,25 @@
     vmem = pl.BlockSpec(memory_space=pltpu.VMEM)
 
     sent = pl.pallas_call(
-        functools.partial(
-            pack_kernel, experts=experts, capacity=capacity, narrow=narrow, piece=piece
-        ),
+        functools.partial(pack_kernel, experts=experts, capacity=capacity),
         out_shape=jax.ShapeDtypeStruct((experts, capacity + piece, narrow), BF16),
-        in_specs=[vmem] * 5,
+        in_specs=[pl.BlockSpec(memory_space=pltpu.HBM)] * 5,
         out_specs=vmem,
-        scratch_shapes=[pltpu.VMEM((block, half), F32)],
+        scratch_shapes=[
+            pltpu.VMEM((n, width), BF16),
+            pltpu.VMEM((top, n), jnp.int32),
+            pltpu.VMEM((1, block), F32),
+            pltpu.VMEM((experts, piece, half), F32),
+            pltpu.VMEM((experts, piece, half), F32),
+            pltpu.VMEM((block, half), F32),
+            pltpu.SemaphoreType.DMA((PARTS + 4,)),
+        ],
         compiler_params=PARAMS,
         name="pack",
-    )(tokens, chosen.T, norm_gain[None, :], gate_master, up_master)
+    )(*(
+        pltpu.with_memory_space_constraint(a, pltpu.HBM)
+        for a in (tokens, chosen.T, norm_gain[None, :], gate_master, up_master)
+    ))
     got = lax.all_to_all(sent, "fs", split_axis=0, concat_axis=0, tiled=True)
     rows = got[:, :capacity, :].reshape(sources * capacity, narrow)
     weights = gather_groups(got[None, :, capacity:, :], groups)

time: 249 us -> 245 us (0.984)
  the two profiles are of different devices: /device:TPU:34 before, /device:TPU:36 now
where the time goes in v2:
time: 245 us
  blocking collectives  150 us (61%)
  waiting for transfers between devices  57.6 us (24%)
  starting transfers between devices  30.6 us (12%)
  Pallas kernels  5.83 us (2%)
    all_to_all x1, blocking collectives, on_device(): got = lax.all_to_all(sent, 'fs', split_axis=0, concat_axis=0, tiled=True)  150 us
    all_to_all x1, waiting for transfers between devices, on_device(): lax.all_to_all(hidden.reshape(sources, capacity, half), 'fs', split_axis=...  41.5 us
    ppermute x2, waiting for transfers between devices, gather_slices(): one = lax.ppermute(one, 'tp', ahead)  10.1 us
    all_to_all x1, starting transfers between devices, on_device(): lax.all_to_all(hidden.reshape(sources, capacity, half), 'fs', split_axis=...  9.11 us
    ppermute x4, starting transfers between devices, gather_slices(): return got + [lax.ppermute(g, 'tp', swap) for g in got]  8.5 us
    ppermute x2, starting transfers between devices, gather_slices(): one = lax.ppermute(one, 'tp', ahead)  6.27 us
    ppermute x1, waiting for transfers between devices, gather_groups(): got.append(lax.ppermute(send, 'grp', table))  5.97 us
  transfers between devices with their start and end apart: 9, of which 3 were waited for; matrix products, arithmetic and copies ran while one was open for 0% of the time, Pallas kernels for 0%

profile of v2, /device:TPU:36, one launch (start us, length us, event | category | flops | bytes accessed | tf_op | source)
XLA Modules:
  0.0 244.9 jit_solution(11286064022546844913)
XLA Ops:
  0.6 2.0 pack.1
  2.6 150.0 %all_to_all.10 = bf16[32,64,256]{2,1,0:T(8,128)(2,1)S(1)} all-to-all(bf16[32,64,256]{2,1,0:T(8,128)(2,1)S(1)} %pack.1), channel_id=1, replica_groups=mesh['grp'=2,'fs'=32,'tp'=8] {'fs'}, dimensions={0} | all-to-all | bytes 2097152 | tf_op jit(solution)/shard_map/all_to_all | solution.py:215
  152.6 0.1 fusion
  152.7 3.3 %collective-permute-start.1 = (bf16[1024,256]{1,0:T(8,128)(2,1)S(1)}, bf16[1024,256]{1,0:T(8,128)(2,1)S(1)}, u32[]{:S(2)}, u32[]{:S(2)}) collective-permute-start(bf16[1024,256]{1,0:T(8,128)(2,1)S(1)} %bitcast.11), channel_id=1, source_target_pairs={{0,2},{1,7},{2,4},{3,1},{4,6},{5,3},{6,0},{7,5},{8,10},{9,15},{10,... | collective-permute-start | bytes 1572872 | tf_op jit(solution)/shard_map/ppermute | solution.py:166
  156.0 2.6 %collective-permute-start.2 = (bf16[1024,256]{1,0:T(8,128)(2,1)S(1)}, bf16[1024,256]{1,0:T(8,128)(2,1)S(1)}, u32[]{:S(2)}, u32[]{:S(2)}) collective-permute-start(bf16[1024,256]{1,0:T(8,128)(2,1)S(1)} %bitcast.12), channel_id=1, source_target_pairs={{0,6},{1,3},{2,0},{3,5},{4,2},{5,7},{6,4},{7,1},{8,14},{9,11},{10,... | collective-permute-start | bytes 1572872 | tf_op jit(solution)/shard_map/ppermute | solution.py:169
  158.6 10.1 %collective-permute-done.1.refs_3_ = bf16[1024,256]{1,0:T(8,128)(2,1)S(1)} collective-permute-done((bf16[1024,256]{1,0:T(8,128)(2,1)S(1)}, bf16[1024,256]{1,0:T(8,128)(2,1)S(1)}, u32[]{:S(2)}, u32[]{:S(2)}) %collective-permute-start.1) | collective-permute-done | bytes 524320 | tf_op jit(solution)/shard_map/ppermute | solution.py:166
  168.8 3.0 %collective-permute-start.3 = (bf16[1024,256]{1,0:T(8,128)(2,1)S(1)}, bf16[1024,256]{1,0:T(8,128)(2,1)S(1)}, u32[]{:S(2)}, u32[]{:S(2)}) collective-permute-start(bf16[1024,256]{1,0:T(8,128)(2,1)S(1)} %collective-permute-done.1.refs_3_), channel_id=1, source_target_pairs={{0,2},{1,7},{2,4},{3,1},{4,6},{5,3},{6,0},{7,5},{8,10},{9,15},{10,... | collective-permute-start | bytes 1572872 | tf_op jit(solution)/shard_map/ppermute | solution.py:166
  171.8 2.0 collective-permute-start.4
  173.7 4.1 %collective-permute-start = (bf16[1,32,32,256]{3,2,1,0:T(8,128)(2,1)S(1)}, bf16[1,32,32,256]{3,2,1,0:T(8,128)(2,1)S(1)}, u32[]{:S(2)}, u32[]{:S(2)}) collective-permute-start(bf16[1,32,32,256]{3,2,1,0:T(8,128)(2,1)S(1)} %get-tuple-element.20.refs_0_), channel_id=1, source_target_pairs={{0,256},{256,0},{1,257},{257,1},{2,258},{258,2},{3,259},{259,3},{4... | collective-permute-start | bytes 1572872 | tf_op jit(solution)/shard_map/ppermute | solution.py:180
  177.8 2.2 collective-permute-start.5
  179.9 0.0 collective-permute-done.2.refs_4_
  179.9 2.2 collective-permute-start.6
  182.2 0.0 collective-permute-done.3.refs_5_
  182.2 2.2 collective-permute-start.7
  184.4 0.0 collective-permute-done.4.refs_6_
  184.4 6.0 %collective-permute-done.refs_1_ = bf16[1,32,32,256]{3,2,1,0:T(8,128)(2,1)S(1)} collective-permute-done((bf16[1,32,32,256]{3,2,1,0:T(8,128)(2,1)S(1)}, bf16[1,32,32,256]{3,2,1,0:T(8,128)(2,1)S(1)}, u32[]{:S(2)}, u32[]{:S(2)}) %collective-permute-start) | collective-permute-done | bytes 524320 | tf_op jit(solution)/shard_map/ppermute | solution.py:180
  190.3 0.0 collective-permute-done.6.refs_8_
  190.3 0.0 collective-permute-done.5.refs_7_
  190.4 0.0 collective-permute-done.7.refs_9_
  190.4 2.4 experts.1
  192.7 0.0 copy-start
  192.7 0.0 copy-start.1
  192.7 9.1 %all-to-all-start.1 = ((bf16[32,32,128]{2,1,0:T(8,128)(2,1)}), bf16[32,32,128]{2,1,0:T(8,128)(2,1)S(1)}, u32[]{:S(2)}, u32[]{:S(2)}) async-start(bf16[32,32,128]{2,1,0:T(8,128)(2,1)} %bitcast.7), calls=%async_computation.1 | async-start | bytes 524288 | tf_op jit(solution)/shard_map/all_to_all | solution.py:234
  201.8 0.0 copy-done
  201.8 0.0 copy-done.1
  201.9 0.4 place.1
  202.3 41.5 %all-to-all-done.1 = bf16[32,32,128]{2,1,0:T(8,128)(2,1)S(1)} async-done(((bf16[32,32,128]{2,1,0:T(8,128)(2,1)}), bf16[32,32,128]{2,1,0:T(8,128)(2,1)S(1)}, u32[]{:S(2)}, u32[]{:S(2)}) %all-to-all-start.1) | async-done | bytes 262176 | tf_op jit(solution)/shard_map/all_to_all | solution.py:234
  243.8 1.1 pick.1
Async XLA Ops:
  152.7 16.0 %collective-permute-start.1 = (bf16[1024,256]{1,0:T(8,128)(2,1)S(1)}, bf16[1024,256]{1,0:T(8,128)(2,1)S(1)}, u32[]{:S(2)}, u32[]{:S(2)}) collective-permute-start(bf16[1024,256]{1,0:T(8,128)(2,1)S(1)} %bitcast.11), channel_id=1, source_target_pairs={{0,2},{1,7},{2,4},{3,1},{4,6},{5,3},{6,0},{7,5},{8,10},{9,15},{10,... | collective-permute-start | bytes 1572872 | tf_op jit(solution)/shard_map/ppermute | solution.py:166
  156.0 23.9 %collective-permute-start.2 = (bf16[1024,256]{1,0:T(8,128)(2,1)S(1)}, bf16[1024,256]{1,0:T(8,128)(2,1)S(1)}, u32[]{:S(2)}, u32[]{:S(2)}) collective-permute-start(bf16[1024,256]{1,0:T(8,128)(2,1)S(1)} %bitcast.12), channel_id=1, source_target_pairs={{0,6},{1,3},{2,0},{3,5},{4,2},{5,7},{6,4},{7,1},{8,14},{9,11},{10,... | collective-permute-start | bytes 1572872 | tf_op jit(solution)/shard_map/ppermute | solution.py:169
  168.8 13.4 %collective-permute-start.3 = (bf16[1024,256]{1,0:T(8,128)(2,1)S(1)}, bf16[1024,256]{1,0:T(8,128)(2,1)S(1)}, u32[]{:S(2)}, u32[]{:S(2)}) collective-permute-start(bf16[1024,256]{1,0:T(8,128)(2,1)S(1)} %collective-permute-done.1.refs_3_), channel_id=1, source_target_pairs={{0,2},{1,7},{2,4},{3,1},{4,6},{5,3},{6,0},{7,5},{8,10},{9,15},{10,... | collective-permute-start | bytes 1572872 | tf_op jit(solution)/shard_map/ppermute | solution.py:166
  171.8 12.6 %collective-permute-start.4 = (bf16[1024,256]{1,0:T(8,128)(2,1)S(1)}, bf16[1024,256]{1,0:T(8,128)(2,1)S(1)}, u32[]{:S(2)}, u32[]{:S(2)}) collective-permute-start(bf16[1024,256]{1,0:T(8,128)(2,1)S(1)} %bitcast.13), channel_id=1, source_target_pairs={{0,1},{1,0},{2,3},{3,2},{4,5},{5,4},{6,7},{7,6},{8,9},{9,8},{10,11... | collective-permute-start | bytes 1572872 | tf_op jit(solution)/shard_map/ppermute | solution.py:171
  173.7 16.6 %collective-permute-start = (bf16[1,32,32,256]{3,2,1,0:T(8,128)(2,1)S(1)}, bf16[1,32,32,256]{3,2,1,0:T(8,128)(2,1)S(1)}, u32[]{:S(2)}, u32[]{:S(2)}) collective-permute-start(bf16[1,32,32,256]{3,2,1,0:T(8,128)(2,1)S(1)} %get-tuple-element.20.refs_0_), channel_id=1, source_target_pairs={{0,256},{256,0},{1,257},{257,1},{2,258},{258,2},{3,259},{259,3},{4... | collective-permute-start | bytes 1572872 | tf_op jit(solution)/shard_map/ppermute | solution.py:180
  177.8 12.6 %collective-permute-start.5 = (bf16[1024,256]{1,0:T(8,128)(2,1)S(1)}, bf16[1024,256]{1,0:T(8,128)(2,1)S(1)}, u32[]{:S(2)}, u32[]{:S(2)}) collective-permute-start(bf16[1024,256]{1,0:T(8,128)(2,1)S(1)} %collective-permute-done.1.refs_3_), channel_id=1, source_target_pairs={{0,1},{1,0},{2,3},{3,2},{4,5},{5,4},{6,7},{7,6},{8,9},{9,8},{10,11... | collective-permute-start | bytes 1572872 | tf_op jit(solution)/shard_map/ppermute | solution.py:171
  179.9 10.4 %collective-permute-start.6 = (bf16[1024,256]{1,0:T(8,128)(2,1)S(1)}, bf16[1024,256]{1,0:T(8,128)(2,1)S(1)}, u32[]{:S(2)}, u32[]{:S(2)}) collective-permute-start(bf16[1024,256]{1,0:T(8,128)(2,1)S(1)} %collective-permute-done.2.refs_4_), channel_id=1, source_target_pairs={{0,1},{1,0},{2,3},{3,2},{4,5},{5,4},{6,7},{7,6},{8,9},{9,8},{10,11... | collective-permute-start | bytes 1572872 | tf_op jit(solution)/shard_map/ppermute | solution.py:171
  182.2 8.2 %collective-permute-start.7 = (bf16[1024,256]{1,0:T(8,128)(2,1)S(1)}, bf16[1024,256]{1,0:T(8,128)(2,1)S(1)}, u32[]{:S(2)}, u32[]{:S(2)}) collective-permute-start(bf16[1024,256]{1,0:T(8,128)(2,1)S(1)} %collective-permute-done.3.refs_5_), channel_id=1, source_target_pairs={{0,1},{1,0},{2,3},{3,2},{4,5},{5,4},{6,7},{7,6},{8,9},{9,8},{10,11... | collective-permute-start | bytes 1572872 | tf_op jit(solution)/shard_map/ppermute | solution.py:171
  192.7 9.1 %copy-start = (s32[256,2]{0,1:T(2,128)S(1)}, s32[256,2]{0,1:T(2,128)}, u32[]{:S(2)}) copy-start(s32[256,2]{0,1:T(2,128)} %param.10) | copy-start | bytes 6148
  192.7 9.1 %copy-start.1 = (f32[256,2]{0,1:T(2,128)S(1)}, f32[256,2]{0,1:T(2,128)}, u32[]{:S(2)}) copy-start(f32[256,2]{0,1:T(2,128)} %param.11) | copy-start | bytes 6148
  192.7 51.0 %all-to-all-start.1 = ((bf16[32,32,128]{2,1,0:T(8,128)(2,1)}), bf16[32,32,128]{2,1,0:T(8,128)(2,1)S(1)}, u32[]{:S(2)}, u32[]{:S(2)}) async-start(bf16[32,32,128]{2,1,0:T(8,128)(2,1)} %bitcast.7), calls=%async_computation.1 | async-start | bytes 524288 | tf_op jit(solution)/shard_map/all_to_all | solution.py:234

commit v3 on v2

--- a/solution.py
+++ b/solution.py
@@ -43,6 +43,7 @@
     n, width = tok.shape
     narrow = out.shape[2]
     piece, half = gat.shape[1:]
+    share = capacity // CORES
     part = n // PARTS
     mine = pl.multiple_of(lax.axis_index("grp") * piece, TILE)
     pairs = [(chosen, cho), (gain, gai)]
@@ -54,17 +55,20 @@
     copies[0].wait()
     named, slot = slots_of(cho[...].astype(F32), experts)
     slot = jnp.where(named > 0, slot, -1.0)
-    pick = slot[:, None, :] == iota((experts, capacity, n), 1).astype(F32)
-    pick = pick.astype(F32).reshape(experts * capacity, n).astype(BF16)
+    first = lax.axis_index("core") * share
+    pick = slot[:, None, :] == (iota((experts, share, n), 1) + first).astype(F32)
+    pick = pick.astype(F32).reshape(experts * share, n).astype(BF16)
     copies[1].wait()
     gains[...] = jnp.broadcast_to(column(gai[...]), gains.shape)
     for c in copies[2 : 2 + PARTS]:
         c.wait()
     x = tok[...].astype(F32)
     scale = lax.rsqrt(jnp.sum(x * x, axis=-1, keepdims=True) / width + 1e-06)
-    at = pl.multiple_of(lax.axis_index("tp") * narrow, narrow)
-    own = (tok[:, pl.ds(at, narrow)].astype(F32) * scale).astype(BF16)
-    out[:, :capacity, :] = dot(pick, own).astype(BF16).reshape(experts, capacity, narrow)
+    for c in range(CORES):
+        at = pl.multiple_of((lax.axis_index("x") * CORES + c) * narrow, narrow)
+        own = (tok[:, pl.ds(at, narrow)].astype(F32) * scale).astype(BF16)
+        rows = dot(pick, own).astype(BF16).reshape(experts, share, narrow)
+        out[:, c * share : (c + 1) * share, :] = rows
     for c in copies[2 + PARTS :]:
         c.wait()
     g = gains[pl.ds(mine, piece), :][None]
@@ -72,33 +76,44 @@
     out[:, capacity:, half:] = (upp[...] * g).astype(BF16)
 
 
-def expert_kernel(*refs, parts, cores):
+def expert_kernel(*refs, parts, chips):
     gate, up, hidden, mixed = refs[-4:]
-    weights, slices = refs[:parts], refs[parts:-4]
+    weights, others, slices = refs[:parts], refs[parts : 2 * parts], refs[2 * parts : -4]
     half = gate.shape[2]
-    total = len(slices)
-    narrow = slices[0].shape[1]
-
+    block = gate.shape[1]
+    slots, narrow = slices[0].shape[1:]
+    share = slots // CORES
+    total = chips * CORES
+    per = gate.shape[0] // total
     piece = weights[0].shape[2]
     mine = lax.axis_index("grp")
-    q = 0
-    for ref in weights:
-        for j in range(ref.shape[0]):
-            at = pl.multiple_of((mine ^ q) * piece, TILE)
-            gate[:, pl.ds(at, piece), :] = ref[j, :, :, :half]
-            up[:, pl.ds(at, piece), :] = ref[j, :, :, half:]
-            q += 1
-    tp = lax.axis_index("tp")
-    per = gate.shape[0] // total
-    for k, where in enumerate(slice_places(total, cores)):
-        at = where(tp) * per
-        mixed[k, :, :half] = gate[pl.ds(at, per)].reshape(narrow, half)
-        mixed[k, :, half:] = up[pl.ds(at, per)].reshape(narrow, half)
-    a = dot(slices[0][...], mixed[0])
-    for k in range(1, total):
-        a = a + dot(slices[k][...], mixed[k])
-    g = a[:, :half]
-    hidden[...] = (g / (1.0 + jnp.exp(-g)) * a[:, half:]).astype(BF16)
+    x = lax.axis_index("x")
+    core = lax.axis_index("core")
+    chip = [place(x, core, chips) for place in chip_places(chips)]
+    for side, group in enumerate((weights, others)):
+        q = 0
+        for ref in group:
+            for j in range(ref.shape[0]):
+                at = pl.multiple_of((mine ^ q) * piece, TILE)
+                if side == 0:
+                    gate[:, pl.ds(at, piece), :] = ref[j, :, :, :half]
+                    up[:, pl.ds(at, piece), :] = ref[j, :, :, half:]
+                for i, c in enumerate(chip):
+                    part = ref[j, pl.ds(c * CORES * per, CORES * per)]
+                    mixed[i, :, pl.ds(at, piece), side * narrow : (side + 1) * narrow] = part
+                q += 1
+    a = None
+    for i, ref in enumerate(slices):
+        for c in range(CORES):
+            rows = ref[:, c * share : (c + 1) * share, :].reshape(-1, narrow)
+            w = mixed[i, c * per : (c + 1) * per].reshape(per * block, CORES * narrow)
+            d = dot(rows, w)
+            a = d if a is None else a + d
+    for side, to in enumerate((core, 1 - core)):
+        g = a[:, side * narrow : side * narrow + half]
+        u = a[:, side * narrow + half : (side + 1) * narrow]
+        h = (g / (1.0 + jnp.exp(-g)) * u).astype(BF16)
+        hidden[:, pl.ds(to, 1)] = h.reshape(hidden.shape[0], 1, share, half)
 
 
 def place_kernel(chosen, affinity, take, share, *, experts, capacity):
@@ -128,47 +143,35 @@
     out[...] = (dot(take[...], back[...]) * share[...]).astype(BF16)
 
 
-def ring_tables(total, cores):
-    def hop(sign):
-        def to(i):
-            turn = sign if i % cores == 0 else -sign
-            return (i + turn * cores) % total
-
-        return [(i, to(i)) for i in range(total)]
-
-    return hop(1), hop(-1), [(i, i ^ 1) for i in range(total)]
-
-
-def slice_places(total, cores):
-    chips = total // cores
-
+def chip_places(chips):
     def away(steps):
-        def place(i):
-            turn = jnp.where(i % cores == 0, -steps, steps)
-            return (i + turn * cores + total) % total
-
-        return place
+        return lambda x, core, n: (x + jnp.where(core == 0, -steps, steps) + n) % n
 
     places = [away(0)]
     for s in range(1, chips // 2 + 1):
         places.append(away(s))
         if s <= (chips - 1) // 2:
             places.append(away(-s))
-    return places + [lambda i, p=p: p(i ^ 1) for p in places]
-
-
-def gather_slices(own, total, cores):
-    ahead, behind, swap = ring_tables(total, cores)
-    chips = total // cores
+    return places
+
+
+def gather_slices(own, chips):
+    def hop(sign):
+        def to(x, c):
+            return (x + (sign if c == 0 else -sign)) % chips
+
+        pairs = [(x, c) for x in range(chips) for c in range(CORES)]
+        return [(x * CORES + c, to(x, c) * CORES + c) for x, c in pairs]
+
     got = [own]
     one = two = own
     for s in range(1, chips // 2 + 1):
-        one = lax.ppermute(one, "tp", ahead)
+        one = lax.ppermute(one, ("x", "core"), hop(1))
         got.append(one)
         if s <= (chips - 1) // 2:
-            two = lax.ppermute(two, "tp", behind)
+            two = lax.ppermute(two, ("x", "core"), hop(-1))
             got.append(two)
-    return got + [lax.ppermute(g, "tp", swap) for g in got]
+    return got
 
 
 def gather_groups(own, groups):
@@ -183,7 +186,8 @@
 
 
 def on_device(tokens, norm_gain, gate_master, up_master, chosen, affinity):
-    groups, sources, total = (lax.axis_size(a) for a in ("grp", "fs", "tp"))
+    groups, sources, chips = (lax.axis_size(a) for a in ("grp", "fs", "x"))
+    total = chips * CORES
     experts, block, half = gate_master.shape
     n, width = tokens.shape
     top = chosen.shape[1]
@@ -213,26 +217,33 @@
         for a in (tokens, chosen.T, norm_gain[None, :], gate_master, up_master)
     ))
     got = lax.all_to_all(sent, "fs", split_axis=0, concat_axis=0, tiled=True)
-    rows = got[:, :capacity, :].reshape(sources * capacity, narrow)
+    rows = got[:, :capacity, :]
     weights = gather_groups(got[None, :, capacity:, :], groups)
-    slices = gather_slices(rows, total, CORES)
+    slices = gather_slices(rows, chips)
+    swap = [(c, 1 - c) for c in range(CORES)]
+    others = [lax.ppermute(w, "core", swap) for w in weights]
+    share = capacity // CORES
 
     gate, up, hidden = pl.pallas_call(
-        functools.partial(expert_kernel, parts=len(weights), cores=CORES),
+        functools.partial(expert_kernel, parts=len(weights), chips=chips),
         out_shape=(
             jax.ShapeDtypeStruct((sources, block, half), BF16),
             jax.ShapeDtypeStruct((sources, block, half), BF16),
-            jax.ShapeDtypeStruct((sources * capacity, half), BF16),
-        ),
-        in_specs=[vmem] * (len(weights) + len(slices)),
+            jax.ShapeDtypeStruct((sources, CORES, share, half), BF16),
+        ),
+        in_specs=[vmem] * (2 * len(weights) + len(slices)),
         out_specs=(vmem, vmem, vmem),
-        scratch_shapes=[pltpu.VMEM((total, narrow, 2 * half), BF16)],
+        scratch_shapes=[pltpu.VMEM((chips, CORES * sources // total, block, CORES * narrow), BF16)],
         compiler_params=PARAMS,
         name="experts",
-    )(*weights, *slices)
+    )(*weights, *others, *slices)
     hidden, choice, ratio = lax.optimization_barrier((hidden, chosen.T, affinity.T))
     back = lax.all_to_all(
-        hidden.reshape(sources, capacity, half), "fs", split_axis=0, concat_axis=0, tiled=True
+        hidden.reshape(sources * CORES, share, half),
+        ("fs", "core"),
+        split_axis=0,
+        concat_axis=0,
+        tiled=True,
     )
     take, share = pl.pallas_call(
         functools.partial(place_kernel, experts=experts, capacity=capacity),
@@ -261,21 +272,24 @@
 
 
 def solution(mesh):
+    groups, sources, total = (mesh.shape[a] for a in ("grp", "fs", "tp"))
+    devices = mesh.devices.reshape(groups, sources, total // CORES, CORES)
+    tp = ("x", "core")
     return jax.shard_map(
         on_device,
-        mesh=mesh,
+        mesh=jax.sharding.Mesh(devices, ("grp", "fs", *tp)),
         in_specs=(
             P(("grp", "fs"), None),
             P("fs"),
-            P(None, "fs", "tp"),
-            P(None, "fs", "tp"),
+            P(None, "fs", tp),
+            P(None, "fs", tp),
             P(("grp", "fs"), None),
             P(("grp", "fs"), None),
         ),
         out_specs=(
-            P(("grp", "fs"), None, "tp"),
-            P(("grp", "fs"), None, "tp"),
-            P(("grp", "fs"), None, "tp"),
+            P(("grp", "fs"), None, tp),
+            P(("grp", "fs"), None, tp),
+            P(("grp", "fs"), None, tp),
         ),
         check_vma=False,
     )

time: 245 us -> 239 us (0.976)
  the two profiles are of different devices: /device:TPU:36 before, /device:TPU:40 now
where the time goes in v3:
time: 239 us; the launch traced here: 238 us
  blocking collectives  150 us (63%)
  waiting for transfers between devices  50.1 us (21%)
  starting transfers between devices  31.2 us (13%)
  Pallas kernels  6 us (3%)
    all_to_all x1, blocking collectives, on_device(): got = lax.all_to_all(sent, 'fs', split_axis=0, concat_axis=0, tiled=True)  150 us
    all_to_all x1, waiting for transfers between devices, on_device(): lax.all_to_all(hidden.reshape(sources * CORES, share, half), ('fs', 'core...  41.3 us
    all_to_all x1, starting transfers between devices, on_device(): lax.all_to_all(hidden.reshape(sources * CORES, share, half), ('fs', 'core...  14 us
    ppermute x2, starting transfers between devices, gather_slices(): one = lax.ppermute(one, ('x', 'core'), hop(1))  7.82 us
    ppermute x2, waiting for transfers between devices, gather_slices(): one = lax.ppermute(one, ('x', 'core'), hop(1))  5.36 us
  transfers between devices with their start and end apart: 7, of which 4 were waited for; matrix products, arithmetic and copies ran while one was open for 0% of the time, Pallas kernels for 0%

profile of v3, /device:TPU:40, one launch (start us, length us, event | category | flops | bytes accessed | tf_op | source)
XLA Modules:
  0.0 238.1 jit_solution(18289471884868733868)
XLA Ops:
  0.6 2.0 pack.1
  2.6 150.0 %all_to_all.10 = bf16[32,64,256]{2,1,0:T(8,128)(2,1)S(1)} all-to-all(bf16[32,64,256]{2,1,0:T(8,128)(2,1)S(1)} %pack.1), channel_id=1, replica_groups=mesh['grp'=2,'fs'=32,'x'=4,'core'=2] {'fs'}, dimensions={0} | all-to-all | bytes 2097152 | tf_op jit(solution)/shard_map/all_to_all | solution.py:219
  152.6 0.1 fusion
  152.7 3.6 %collective-permute-start.3 = (bf16[32,32,256]{2,1,0:T(8,128)(2,1)S(1)}, bf16[32,32,256]{2,1,0:T(8,128)(2,1)S(1)}, u32[]{:S(2)}, u32[]{:S(2)}) collective-permute-start(bf16[32,32,256]{2,1,0:T(8,128)(2,1)S(1)} %get-tuple-element.19.refs_4_), channel_id=1, source_target_pairs={{0,2},{1,7},{2,4},{3,1},{4,6},{5,3},{6,0},{7,5},{8,10},{9,15},{10,... | collective-permute-start | bytes 1572872 | tf_op jit(solution)/shard_map/ppermute | solution.py:169
  156.3 2.0 collective-permute-start
  158.3 3.5 %collective-permute-start.4 = (bf16[32,32,256]{2,1,0:T(8,128)(2,1)S(1)}, bf16[32,32,256]{2,1,0:T(8,128)(2,1)S(1)}, u32[]{:S(2)}, u32[]{:S(2)}) collective-permute-start(bf16[32,32,256]{2,1,0:T(8,128)(2,1)S(1)} %get-tuple-element.19.refs_4_), channel_id=1, source_target_pairs={{0,6},{1,3},{2,0},{3,5},{4,2},{5,7},{6,4},{7,1},{8,14},{9,11},{10,... | collective-permute-start | bytes 1572872 | tf_op jit(solution)/shard_map/ppermute | solution.py:172
  161.8 2.0 collective-permute-start.1
  163.8 1.5 collective-permute-done.3.refs_5_
  165.2 4.3 %collective-permute-start.5 = (bf16[32,32,256]{2,1,0:T(8,128)(2,1)S(1)}, bf16[32,32,256]{2,1,0:T(8,128)(2,1)S(1)}, u32[]{:S(2)}, u32[]{:S(2)}) collective-permute-start(bf16[32,32,256]{2,1,0:T(8,128)(2,1)S(1)} %collective-permute-done.3.refs_5_), channel_id=1, source_target_pairs={{0,2},{1,7},{2,4},{3,1},{4,6},{5,3},{6,0},{7,5},{8,10},{9,15},{10,... | collective-permute-start | bytes 1572872 | tf_op jit(solution)/shard_map/ppermute | solution.py:169
  169.5 3.4 %collective-permute-done.refs_1_ = bf16[1,32,32,256]{3,2,1,0:T(8,128)(2,1)S(1)} collective-permute-done((bf16[1,32,32,256]{3,2,1,0:T(8,128)(2,1)S(1)}, bf16[1,32,32,256]{3,2,1,0:T(8,128)(2,1)S(1)}, u32[]{:S(2)}, u32[]{:S(2)}) %collective-permute-start) | collective-permute-done | bytes 524320 | tf_op jit(solution)/shard_map/ppermute | solution.py:183
  172.9 1.9 collective-permute-start.2
  174.8 0.0 collective-permute-done.4.refs_6_
  174.9 0.0 collective-permute-done.1.refs_2_
  174.9 3.9 %collective-permute-done.5.refs_7_ = bf16[32,32,256]{2,1,0:T(8,128)(2,1)S(1)} collective-permute-done((bf16[32,32,256]{2,1,0:T(8,128)(2,1)S(1)}, bf16[32,32,256]{2,1,0:T(8,128)(2,1)S(1)}, u32[]{:S(2)}, u32[]{:S(2)}) %collective-permute-start.5) | collective-permute-done | bytes 524320 | tf_op jit(solution)/shard_map/ppermute | solution.py:169
  178.8 0.0 collective-permute-done.2.refs_3_
  178.8 2.5 %experts.1 = (bf16[32,64,128]{2,1,0:T(8,128)(2,1)}, bf16[32,64,128]{2,1,0:T(8,128)(2,1)}, bf16[32,2,16,128]{3,2,1,0:T(8,128)(2,1)}) custom-call(bf16[1,32,32,256]{3,2,1,0:T(8,128)(2,1)S(1)} %get-tuple-element.20.refs_0_, bf16[1,32,32,256]{3,2,1,0:T(8,128)(2,1)S(1)} %collective-permute-done.refs_1_, ...), custom_call_target="tpu_custom_call" | custom-call | tf_op jit(solution)/shard_map/experts/pallas_call | solution.py:227
  181.3 0.0 copy-start
  181.3 0.0 copy-start.1
  181.3 14.0 %all-to-all-start.1 = ((bf16[64,16,128]{2,1,0:T(8,128)(2,1)}), bf16[64,16,128]{2,1,0:T(8,128)(2,1)S(1)}, u32[]{:S(2)}, u32[]{:S(2)}) async-start(bf16[64,16,128]{2,1,0:T(8,128)(2,1)} %bitcast.6), calls=%async_computation.1 | async-start | bytes 524288 | tf_op jit(solution)/shard_map/all_to_all | solution.py:241
  195.3 0.0 copy-done
  195.3 0.0 copy-done.1
  195.3 0.4 place.1
  195.7 41.3 %all-to-all-done.1 = bf16[64,16,128]{2,1,0:T(8,128)(2,1)S(1)} async-done(((bf16[64,16,128]{2,1,0:T(8,128)(2,1)}), bf16[64,16,128]{2,1,0:T(8,128)(2,1)S(1)}, u32[]{:S(2)}, u32[]{:S(2)}) %all-to-all-start.1) | async-done | bytes 262176 | tf_op jit(solution)/shard_map/all_to_all | solution.py:241
  237.0 1.1 pick.1
Async XLA Ops:
  152.7 12.5 %collective-permute-start.3 = (bf16[32,32,256]{2,1,0:T(8,128)(2,1)S(1)}, bf16[32,32,256]{2,1,0:T(8,128)(2,1)S(1)}, u32[]{:S(2)}, u32[]{:S(2)}) collective-permute-start(bf16[32,32,256]{2,1,0:T(8,128)(2,1)S(1)} %get-tuple-element.19.refs_4_), channel_id=1, source_target_pairs={{0,2},{1,7},{2,4},{3,1},{4,6},{5,3},{6,0},{7,5},{8,10},{9,15},{10,... | collective-permute-start | bytes 1572872 | tf_op jit(solution)/shard_map/ppermute | solution.py:169
  156.3 16.6 %collective-permute-start = (bf16[1,32,32,256]{3,2,1,0:T(8,128)(2,1)S(1)}, bf16[1,32,32,256]{3,2,1,0:T(8,128)(2,1)S(1)}, u32[]{:S(2)}, u32[]{:S(2)}) collective-permute-start(bf16[1,32,32,256]{3,2,1,0:T(8,128)(2,1)S(1)} %get-tuple-element.20.refs_0_), channel_id=1, source_target_pairs={{0,256},{256,0},{1,257},{257,1},{2,258},{258,2},{3,259},{259,3},{4... | collective-permute-start | bytes 1572872 | tf_op jit(solution)/shard_map/ppermute | solution.py:183
  158.3 16.6 %collective-permute-start.4 = (bf16[32,32,256]{2,1,0:T(8,128)(2,1)S(1)}, bf16[32,32,256]{2,1,0:T(8,128)(2,1)S(1)}, u32[]{:S(2)}, u32[]{:S(2)}) collective-permute-start(bf16[32,32,256]{2,1,0:T(8,128)(2,1)S(1)} %get-tuple-element.19.refs_4_), channel_id=1, source_target_pairs={{0,6},{1,3},{2,0},{3,5},{4,2},{5,7},{6,4},{7,1},{8,14},{9,11},{10,... | collective-permute-start | bytes 1572872 | tf_op jit(solution)/shard_map/ppermute | solution.py:172
  161.8 13.0 %collective-permute-start.1 = (bf16[1,32,32,256]{3,2,1,0:T(8,128)(2,1)S(1)}, bf16[1,32,32,256]{3,2,1,0:T(8,128)(2,1)S(1)}, u32[]{:S(2)}, u32[]{:S(2)}) collective-permute-start(bf16[1,32,32,256]{3,2,1,0:T(8,128)(2,1)S(1)} %get-tuple-element.20.refs_0_), channel_id=1, source_target_pairs={{0,1},{1,0},{2,3},{3,2},{4,5},{5,4},{6,7},{7,6},{8,9},{9,8},{10,11... | collective-permute-start | bytes 1572872 | tf_op jit(solution)/shard_map/ppermute | solution.py:224
  165.2 13.5 %collective-permute-start.5 = (bf16[32,32,256]{2,1,0:T(8,128)(2,1)S(1)}, bf16[32,32,256]{2,1,0:T(8,128)(2,1)S(1)}, u32[]{:S(2)}, u32[]{:S(2)}) collective-permute-start(bf16[32,32,256]{2,1,0:T(8,128)(2,1)S(1)} %collective-permute-done.3.refs_5_), channel_id=1, source_target_pairs={{0,2},{1,7},{2,4},{3,1},{4,6},{5,3},{6,0},{7,5},{8,10},{9,15},{10,... | collective-permute-start | bytes 1572872 | tf_op jit(solution)/shard_map/ppermute | solution.py:169
  172.9 5.9 %collective-permute-start.2 = (bf16[1,32,32,256]{3,2,1,0:T(8,128)(2,1)S(1)}, bf16[1,32,32,256]{3,2,1,0:T(8,128)(2,1)S(1)}, u32[]{:S(2)}, u32[]{:S(2)}) collective-permute-start(bf16[1,32,32,256]{3,2,1,0:T(8,128)(2,1)S(1)} %collective-permute-done.refs_1_), channel_id=1, source_target_pairs={{0,1},{1,0},{2,3},{3,2},{4,5},{5,4},{6,7},{7,6},{8,9},{9,8},{10,11... | collective-permute-start | bytes 1572872 | tf_op jit(solution)/shard_map/ppermute | solution.py:224
  181.3 14.0 %copy-start = (s32[256,2]{0,1:T(2,128)S(1)}, s32[256,2]{0,1:T(2,128)}, u32[]{:S(2)}) copy-start(s32[256,2]{0,1:T(2,128)} %param.10) | copy-start | bytes 6148
  181.3 14.0 %copy-start.1 = (f32[256,2]{0,1:T(2,128)S(1)}, f32[256,2]{0,1:T(2,128)}, u32[]{:S(2)}) copy-start(f32[256,2]{0,1:T(2,128)} %param.11) | copy-start | bytes 6148
  181.3 55.8 %all-to-all-start.1 = ((bf16[64,16,128]{2,1,0:T(8,128)(2,1)}), bf16[64,16,128]{2,1,0:T(8,128)(2,1)S(1)}, u32[]{:S(2)}, u32[]{:S(2)}) async-start(bf16[64,16,128]{2,1,0:T(8,128)(2,1)} %bitcast.6), calls=%async_computation.1 | async-start | bytes 524288 | tf_op jit(solution)/shard_map/all_to_all | solution.py:241

commit v4 on v3

--- a/solution.py
+++ b/solution.py
@@ -76,15 +76,12 @@
     out[:, capacity:, half:] = (upp[...] * g).astype(BF16)
 
 
-def expert_kernel(*refs, parts, chips):
-    gate, up, hidden, mixed = refs[-4:]
-    weights, others, slices = refs[:parts], refs[parts : 2 * parts], refs[2 * parts : -4]
+def assemble_kernel(*refs, parts, chips):
+    gate, up, mixed = refs[-3:]
+    weights, others = refs[:parts], refs[parts:-3]
     half = gate.shape[2]
-    block = gate.shape[1]
-    slots, narrow = slices[0].shape[1:]
-    share = slots // CORES
-    total = chips * CORES
-    per = gate.shape[0] // total
+    narrow = 2 * half
+    rows = mixed.shape[1]
     piece = weights[0].shape[2]
     mine = lax.axis_index("grp")
     x = lax.axis_index("x")
@@ -99,9 +96,19 @@
                     gate[:, pl.ds(at, piece), :] = ref[j, :, :, :half]
                     up[:, pl.ds(at, piece), :] = ref[j, :, :, half:]
                 for i, c in enumerate(chip):
-                    part = ref[j, pl.ds(c * CORES * per, CORES * per)]
+                    part = ref[j, pl.ds(c * rows, rows)]
                     mixed[i, :, pl.ds(at, piece), side * narrow : (side + 1) * narrow] = part
                 q += 1
+
+
+def expert_kernel(mixed, *refs):
+    hidden, slices = refs[-1], refs[:-1]
+    half = hidden.shape[3]
+    slots, narrow = slices[0].shape[1:]
+    share = slots // CORES
+    per = mixed.shape[1] // CORES
+    block = mixed.shape[2]
+    core = lax.axis_index("core")
     a = None
     for i, ref in enumerate(slices):
         for c in range(CORES):
@@ -224,19 +231,26 @@
     others = [lax.ppermute(w, "core", swap) for w in weights]
     share = capacity // CORES
 
-    gate, up, hidden = pl.pallas_call(
-        functools.partial(expert_kernel, parts=len(weights), chips=chips),
+    gate, up, mixed = pl.pallas_call(
+        functools.partial(assemble_kernel, parts=len(weights), chips=chips),
         out_shape=(
             jax.ShapeDtypeStruct((sources, block, half), BF16),
             jax.ShapeDtypeStruct((sources, block, half), BF16),
-            jax.ShapeDtypeStruct((sources, CORES, share, half), BF16),
+            pltpu.VMEM((chips, CORES * sources // total, block, CORES * narrow), BF16),
         ),
-        in_specs=[vmem] * (2 * len(weights) + len(slices)),
+        in_specs=[vmem] * (2 * len(weights)),
         out_specs=(vmem, vmem, vmem),
-        scratch_shapes=[pltpu.VMEM((chips, CORES * sources // total, block, CORES * narrow), BF16)],
+        compiler_params=PARAMS,
+        name="assemble",
+    )(*weights, *others)
+    hidden = pl.pallas_call(
+        expert_kernel,
+        out_shape=pltpu.VMEM((sources, CORES, share, half), BF16),
+        in_specs=[vmem] * (1 + len(slices)),
+        out_specs=vmem,
         compiler_params=PARAMS,
         name="experts",
-    )(*weights, *others, *slices)
+    )(mixed, *slices)
     hidden, choice, ratio = lax.optimization_barrier((hidden, chosen.T, affinity.T))
     back = lax.all_to_all(
         hidden.reshape(sources * CORES, share, half),

time: 239 us -> 243 us (1.017)
  the two profiles are of different devices: /device:TPU:40 before, /device:TPU:46 now
where the time goes in v4:
time: 243 us; the launch traced here: 242 us
  blocking collectives  150 us (62%)
  waiting for transfers between devices  58.7 us (24%)
  starting transfers between devices  25.9 us (11%)
  Pallas kernels  6.75 us (3%)
    all_to_all x1, blocking collectives, on_device(): got = lax.all_to_all(sent, 'fs', split_axis=0, concat_axis=0, tiled=True)  150 us
    all_to_all x1, waiting for transfers between devices, on_device(): lax.all_to_all(hidden.reshape(sources * CORES, share, half), ('fs', 'core...  41.3 us
    all_to_all x1, starting transfers between devices, on_device(): lax.all_to_all(hidden.reshape(sources * CORES, share, half), ('fs', 'core...  11 us
    ppermute x1, waiting for transfers between devices, gather_groups(): got.append(lax.ppermute(send, 'grp', table))  9.41 us
    ppermute x1, waiting for transfers between devices, gather_slices(): two = lax.ppermute(two, ('x', 'core'), hop(-1))  7.97 us
    ppermute x2, starting transfers between devices, gather_slices(): one = lax.ppermute(one, ('x', 'core'), hop(1))  6.49 us
  transfers between devices with their start and end apart: 7, of which 3 were waited for; matrix products, arithmetic and copies ran while one was open for 0% of the time, Pallas kernels for 1%

profile of v4, /device:TPU:46, one launch (start us, length us, event | category | flops | bytes accessed | tf_op | source)
XLA Modules:
  0.0 242.3 jit_solution(9244150123737393524)
XLA Ops:
  0.6 2.0 pack.1
  2.6 150.0 %all_to_all.10 = bf16[32,64,256]{2,1,0:T(8,128)(2,1)S(1)} all-to-all(bf16[32,64,256]{2,1,0:T(8,128)(2,1)S(1)} %pack.1), channel_id=1, replica_groups=mesh['grp'=2,'fs'=32,'x'=4,'core'=2] {'fs'}, dimensions={0} | all-to-all | bytes 2097152 | tf_op jit(solution)/shard_map/all_to_all | solution.py:226
  152.6 0.1 fusion
  152.7 2.0 collective-permute-start
  154.7 2.0 collective-permute-start.3
  156.7 2.0 collective-permute-start.1
  158.7 9.4 %collective-permute-done.refs_1_ = bf16[1,32,32,256]{3,2,1,0:T(8,128)(2,1)S(1)} collective-permute-done((bf16[1,32,32,256]{3,2,1,0:T(8,128)(2,1)S(1)}, bf16[1,32,32,256]{3,2,1,0:T(8,128)(2,1)S(1)}, u32[]{:S(2)}, u32[]{:S(2)}) %collective-permute-start) | collective-permute-done | bytes 524320 | tf_op jit(solution)/shard_map/ppermute | solution.py:190
  168.1 1.9 collective-permute-start.2
  170.0 2.6 %collective-permute-start.4 = (bf16[32,32,256]{2,1,0:T(8,128)(2,1)S(1)}, bf16[32,32,256]{2,1,0:T(8,128)(2,1)S(1)}, u32[]{:S(2)}, u32[]{:S(2)}) collective-permute-start(bf16[32,32,256]{2,1,0:T(8,128)(2,1)S(1)} %get-tuple-element.19.refs_0_), channel_id=1, source_target_pairs={{0,6},{1,3},{2,0},{3,5},{4,2},{5,7},{6,4},{7,1},{8,14},{9,11},{10,... | collective-permute-start | bytes 1572872 | tf_op jit(solution)/shard_map/ppermute | solution.py:179
  172.7 0.0 collective-permute-done.3.refs_1_
  172.7 4.5 %collective-permute-start.5 = (bf16[32,32,256]{2,1,0:T(8,128)(2,1)S(1)}, bf16[32,32,256]{2,1,0:T(8,128)(2,1)S(1)}, u32[]{:S(2)}, u32[]{:S(2)}) collective-permute-start(bf16[32,32,256]{2,1,0:T(8,128)(2,1)S(1)} %collective-permute-done.3.refs_1_), channel_id=1, source_target_pairs={{0,2},{1,7},{2,4},{3,1},{4,6},{5,3},{6,0},{7,5},{8,10},{9,15},{10,... | collective-permute-start | bytes 1572872 | tf_op jit(solution)/shard_map/ppermute | solution.py:176
  177.2 0.0 collective-permute-done.1.refs_2_
  177.2 0.0 collective-permute-done.2.refs_3_
  177.2 1.3 assemble.1
  178.5 8.0 %collective-permute-done.4.refs_2_ = bf16[32,32,256]{2,1,0:T(8,128)(2,1)S(1)} collective-permute-done((bf16[32,32,256]{2,1,0:T(8,128)(2,1)S(1)}, bf16[32,32,256]{2,1,0:T(8,128)(2,1)S(1)}, u32[]{:S(2)}, u32[]{:S(2)}) %collective-permute-start.4) | collective-permute-done | bytes 524320 | tf_op jit(solution)/shard_map/ppermute | solution.py:179
  186.5 0.0 collective-permute-done.5.refs_3_
  186.5 0.0 copy-start
  186.5 0.0 copy-start.1
  186.5 2.0 experts.1
  188.4 11.0 %all-to-all-start.1 = ((bf16[64,16,128]{2,1,0:T(8,128)(2,1)}), bf16[64,16,128]{2,1,0:T(8,128)(2,1)S(1)}, u32[]{:S(2)}, u32[]{:S(2)}) async-start(bf16[64,16,128]{2,1,0:T(8,128)(2,1)} %bitcast.6), calls=%async_computation.1 | async-start | bytes 524288 | tf_op jit(solution)/shard_map/all_to_all | solution.py:255
  199.4 0.0 copy-done
  199.4 0.0 copy-done.1
  199.4 0.4 place.1
  199.8 41.3 %all-to-all-done.1 = bf16[64,16,128]{2,1,0:T(8,128)(2,1)S(1)} async-done(((bf16[64,16,128]{2,1,0:T(8,128)(2,1)}), bf16[64,16,128]{2,1,0:T(8,128)(2,1)S(1)}, u32[]{:S(2)}, u32[]{:S(2)}) %all-to-all-start.1) | async-done | bytes 262176 | tf_op jit(solution)/shard_map/all_to_all | solution.py:255
  241.2 1.1 pick.1
Async XLA Ops:
  152.7 15.3 %collective-permute-start = (bf16[1,32,32,256]{3,2,1,0:T(8,128)(2,1)S(1)}, bf16[1,32,32,256]{3,2,1,0:T(8,128)(2,1)S(1)}, u32[]{:S(2)}, u32[]{:S(2)}) collective-permute-start(bf16[1,32,32,256]{3,2,1,0:T(8,128)(2,1)S(1)} %get-tuple-element.20.refs_0_), channel_id=1, source_target_pairs={{0,256},{256,0},{1,257},{257,1},{2,258},{258,2},{3,259},{259,3},{4... | collective-permute-start | bytes 1572872 | tf_op jit(solution)/shard_map/ppermute | solution.py:190
  154.7 18.0 %collective-permute-start.3 = (bf16[32,32,256]{2,1,0:T(8,128)(2,1)S(1)}, bf16[32,32,256]{2,1,0:T(8,128)(2,1)S(1)}, u32[]{:S(2)}, u32[]{:S(2)}) collective-permute-start(bf16[32,32,256]{2,1,0:T(8,128)(2,1)S(1)} %get-tuple-element.19.refs_0_), channel_id=1, source_target_pairs={{0,2},{1,7},{2,4},{3,1},{4,6},{5,3},{6,0},{7,5},{8,10},{9,15},{10,... | collective-permute-start | bytes 1572872 | tf_op jit(solution)/shard_map/ppermute | solution.py:176
  156.7 20.5 %collective-permute-start.1 = (bf16[1,32,32,256]{3,2,1,0:T(8,128)(2,1)S(1)}, bf16[1,32,32,256]{3,2,1,0:T(8,128)(2,1)S(1)}, u32[]{:S(2)}, u32[]{:S(2)}) collective-permute-start(bf16[1,32,32,256]{3,2,1,0:T(8,128)(2,1)S(1)} %get-tuple-element.20.refs_0_), channel_id=1, source_target_pairs={{0,1},{1,0},{2,3},{3,2},{4,5},{5,4},{6,7},{7,6},{8,9},{9,8},{10,11... | collective-permute-start | bytes 1572872 | tf_op jit(solution)/shard_map/ppermute | solution.py:231
  168.1 9.1 %collective-permute-start.2 = (bf16[1,32,32,256]{3,2,1,0:T(8,128)(2,1)S(1)}, bf16[1,32,32,256]{3,2,1,0:T(8,128)(2,1)S(1)}, u32[]{:S(2)}, u32[]{:S(2)}) collective-permute-start(bf16[1,32,32,256]{3,2,1,0:T(8,128)(2,1)S(1)} %collective-permute-done.refs_1_), channel_id=1, source_target_pairs={{0,1},{1,0},{2,3},{3,2},{4,5},{5,4},{6,7},{7,6},{8,9},{9,8},{10,11... | collective-permute-start | bytes 1572872 | tf_op jit(solution)/shard_map/ppermute | solution.py:231
  170.0 16.4 %collective-permute-start.4 = (bf16[32,32,256]{2,1,0:T(8,128)(2,1)S(1)}, bf16[32,32,256]{2,1,0:T(8,128)(2,1)S(1)}, u32[]{:S(2)}, u32[]{:S(2)}) collective-permute-start(bf16[32,32,256]{2,1,0:T(8,128)(2,1)S(1)} %get-tuple-element.19.refs_0_), channel_id=1, source_target_pairs={{0,6},{1,3},{2,0},{3,5},{4,2},{5,7},{6,4},{7,1},{8,14},{9,11},{10,... | collective-permute-start | bytes 1572872 | tf_op jit(solution)/shard_map/ppermute | solution.py:179
  172.7 13.8 %collective-permute-start.5 = (bf16[32,32,256]{2,1,0:T(8,128)(2,1)S(1)}, bf16[32,32,256]{2,1,0:T(8,128)(2,1)S(1)}, u32[]{:S(2)}, u32[]{:S(2)}) collective-permute-start(bf16[32,32,256]{2,1,0:T(8,128)(2,1)S(1)} %collective-permute-done.3.refs_1_), channel_id=1, source_target_pairs={{0,2},{1,7},{2,4},{3,1},{4,6},{5,3},{6,0},{7,5},{8,10},{9,15},{10,... | collective-permute-start | bytes 1572872 | tf_op jit(solution)/shard_map/ppermute | solution.py:176
  186.5 12.9 %copy-start = (s32[256,2]{0,1:T(2,128)S(1)}, s32[256,2]{0,1:T(2,128)}, u32[]{:S(2)}) copy-start(s32[256,2]{0,1:T(2,128)} %param.10) | copy-start | bytes 6148
  186.5 13.0 %copy-start.1 = (f32[256,2]{0,1:T(2,128)S(1)}, f32[256,2]{0,1:T(2,128)}, u32[]{:S(2)}) copy-start(f32[256,2]{0,1:T(2,128)} %param.11) | copy-start | bytes 6148
  188.4 52.7 %all-to-all-start.1 = ((bf16[64,16,128]{2,1,0:T(8,128)(2,1)}), bf16[64,16,128]{2,1,0:T(8,128)(2,1)S(1)}, u32[]{:S(2)}, u32[]{:S(2)}) async-start(bf16[64,16,128]{2,1,0:T(8,128)(2,1)} %bitcast.6), calls=%async_computation.1 | async-start | bytes 524288 | tf_op jit(solution)/shard_map/all_to_all | solution.py:255

commit v5 on v4

--- a/solution.py
+++ b/solution.py
@@ -120,7 +120,10 @@
         g = a[:, side * narrow : side * narrow + half]
         u = a[:, side * narrow + half : (side + 1) * narrow]
         h = (g / (1.0 + jnp.exp(-g)) * u).astype(BF16)
-        hidden[:, pl.ds(to, 1)] = h.reshape(hidden.shape[0], 1, share, half)
+        h = h.reshape(hidden.shape[0], 1, share, half)
+        turn = hidden.shape[0] // 2
+        hidden[:turn, pl.ds(to, 1)] = h[turn:]
+        hidden[turn:, pl.ds(to, 1)] = h[:turn]
 
 
 def place_kernel(chosen, affinity, take, share, *, experts, capacity):
@@ -129,6 +132,7 @@
     choice = chosen[...].astype(F32)
     _, slot = slots_of(choice, experts)
     expert = iota((experts, n), 0).astype(F32)
+    turn = experts // 2
     a = affinity[...]
     part = a / jnp.sum(a, axis=0, keepdims=True)
     line = iota((lines, n), 0)
@@ -137,7 +141,8 @@
     of = jnp.zeros((lines, n), F32)
     for k in range(top):
         c = choice[k : k + 1, :]
-        goal = jnp.sum(jnp.where(c == expert, slot, 0.0), axis=0, keepdims=True) + c * capacity
+        place = jnp.where(c < turn, c + turn, c - turn)
+        goal = jnp.sum(jnp.where(c == expert, slot, 0.0), axis=0, keepdims=True) + place * capacity
         this = here & (line % top == k)
         at = jnp.where(this, goal, at)
         of = jnp.where(this, part[k : k + 1, :], of)
@@ -252,11 +257,14 @@
         name="experts",
     )(mixed, *slices)
     hidden, choice, ratio = lax.optimization_barrier((hidden, chosen.T, affinity.T))
+    turn = sources // 2
+    order = [(z + turn) % sources * CORES + c for z in range(sources) for c in range(CORES)]
     back = lax.all_to_all(
         hidden.reshape(sources * CORES, share, half),
         ("fs", "core"),
         split_axis=0,
         concat_axis=0,
+        axis_index_groups=[order],
         tiled=True,
     )
     take, share = pl.pallas_call(

time: 243 us -> 240 us (0.988)
  the two profiles are of different devices: /device:TPU:46 before, /device:TPU:33 now
where the time goes in v5:
time: 240 us
  blocking collectives  151 us (63%)
  starting transfers between devices  45.8 us (19%)
  waiting for transfers between devices  35.7 us (15%)
  Pallas kernels  6.76 us (3%)
    all_to_all x1, blocking collectives, on_device(): got = lax.all_to_all(sent, 'fs', split_axis=0, concat_axis=0, tiled=True)  151 us
    all_to_all x1, starting transfers between devices, on_device(): lax.all_to_all(hidden.reshape(sources * CORES, share, half), ('fs', 'core...  25.1 us
    all_to_all x1, waiting for transfers between devices, on_device(): lax.all_to_all(hidden.reshape(sources * CORES, share, half), ('fs', 'core...  22.3 us
    ppermute x2, starting transfers between devices, gather_slices(): one = lax.ppermute(one, ('x', 'core'), hop(1))  8.31 us
    ppermute x2, starting transfers between devices, on_device(): others = [lax.ppermute(w, 'core', swap) for w in weights]  5.38 us
    ppermute x2, waiting for transfers between devices, gather_slices(): one = lax.ppermute(one, ('x', 'core'), hop(1))  5.1 us
  transfers between devices with their start and end apart: 7, of which 4 were waited for; matrix products, arithmetic and copies ran while one was open for 0% of the time, Pallas kernels for 1%

profile of v5, /device:TPU:33, one launch (start us, length us, event | category | flops | bytes accessed | tf_op | source)
XLA Modules:
  0.0 239.7 jit_solution(4698236517509273953)
XLA Ops:
  0.6 2.0 pack.1
  2.6 150.5 %all_to_all.10 = bf16[32,64,256]{2,1,0:T(8,128)(2,1)S(1)} all-to-all(bf16[32,64,256]{2,1,0:T(8,128)(2,1)S(1)} %pack.1), channel_id=1, replica_groups=mesh['grp'=2,'fs'=32,'x'=4,'core'=2] {'fs'}, dimensions={0} | all-to-all | bytes 2097152 | tf_op jit(solution)/shard_map/all_to_all | solution.py:231
  153.1 0.1 fusion
  153.2 3.8 %collective-permute-start = (bf16[1,32,32,256]{3,2,1,0:T(8,128)(2,1)S(1)}, bf16[1,32,32,256]{3,2,1,0:T(8,128)(2,1)S(1)}, u32[]{:S(2)}, u32[]{:S(2)}) collective-permute-start(bf16[1,32,32,256]{3,2,1,0:T(8,128)(2,1)S(1)} %get-tuple-element.20.refs_0_), channel_id=1, source_target_pairs={{0,256},{256,0},{1,257},{257,1},{2,258},{258,2},{3,259},{259,3},{4... | collective-permute-start | bytes 1572872 | tf_op jit(solution)/shard_map/ppermute | solution.py:195
  157.0 4.8 %collective-permute-start.3 = (bf16[32,32,256]{2,1,0:T(8,128)(2,1)S(1)}, bf16[32,32,256]{2,1,0:T(8,128)(2,1)S(1)}, u32[]{:S(2)}, u32[]{:S(2)}) collective-permute-start(bf16[32,32,256]{2,1,0:T(8,128)(2,1)S(1)} %get-tuple-element.19.refs_0_), channel_id=1, source_target_pairs={{0,2},{1,7},{2,4},{3,1},{4,6},{5,3},{6,0},{7,5},{8,10},{9,15},{10,... | collective-permute-start | bytes 1572872 | tf_op jit(solution)/shard_map/ppermute | solution.py:181
  161.8 2.0 collective-permute-start.1
  163.8 4.6 %collective-permute-done.refs_1_ = bf16[1,32,32,256]{3,2,1,0:T(8,128)(2,1)S(1)} collective-permute-done((bf16[1,32,32,256]{3,2,1,0:T(8,128)(2,1)S(1)}, bf16[1,32,32,256]{3,2,1,0:T(8,128)(2,1)S(1)}, u32[]{:S(2)}, u32[]{:S(2)}) %collective-permute-start) | collective-permute-done | bytes 524320 | tf_op jit(solution)/shard_map/ppermute | solution.py:195
  168.4 3.4 %collective-permute-start.2 = (bf16[1,32,32,256]{3,2,1,0:T(8,128)(2,1)S(1)}, bf16[1,32,32,256]{3,2,1,0:T(8,128)(2,1)S(1)}, u32[]{:S(2)}, u32[]{:S(2)}) collective-permute-start(bf16[1,32,32,256]{3,2,1,0:T(8,128)(2,1)S(1)} %collective-permute-done.refs_1_), channel_id=1, source_target_pairs={{0,1},{1,0},{2,3},{3,2},{4,5},{5,4},{6,7},{7,6},{8,9},{9,8},{10,11... | collective-permute-start | bytes 1572872 | tf_op jit(solution)/shard_map/ppermute | solution.py:236
  171.8 3.3 %collective-permute-start.4 = (bf16[32,32,256]{2,1,0:T(8,128)(2,1)S(1)}, bf16[32,32,256]{2,1,0:T(8,128)(2,1)S(1)}, u32[]{:S(2)}, u32[]{:S(2)}) collective-permute-start(bf16[32,32,256]{2,1,0:T(8,128)(2,1)S(1)} %get-tuple-element.19.refs_0_), channel_id=1, source_target_pairs={{0,6},{1,3},{2,0},{3,5},{4,2},{5,7},{6,4},{7,1},{8,14},{9,11},{10,... | collective-permute-start | bytes 1572872 | tf_op jit(solution)/shard_map/ppermute | solution.py:184
  175.1 0.0 collective-permute-done.3.refs_1_
  175.1 3.5 %collective-permute-start.5 = (bf16[32,32,256]{2,1,0:T(8,128)(2,1)S(1)}, bf16[32,32,256]{2,1,0:T(8,128)(2,1)S(1)}, u32[]{:S(2)}, u32[]{:S(2)}) collective-permute-start(bf16[32,32,256]{2,1,0:T(8,128)(2,1)S(1)} %collective-permute-done.3.refs_1_), channel_id=1, source_target_pairs={{0,2},{1,7},{2,4},{3,1},{4,6},{5,3},{6,0},{7,5},{8,10},{9,15},{10,... | collective-permute-start | bytes 1572872 | tf_op jit(solution)/shard_map/ppermute | solution.py:181
  178.6 0.0 collective-permute-done.1.refs_2_
  178.6 0.0 collective-permute-done.2.refs_3_
  178.6 1.3 assemble.1
  179.9 3.8 %collective-permute-done.4.refs_2_ = bf16[32,32,256]{2,1,0:T(8,128)(2,1)S(1)} collective-permute-done((bf16[32,32,256]{2,1,0:T(8,128)(2,1)S(1)}, bf16[32,32,256]{2,1,0:T(8,128)(2,1)S(1)}, u32[]{:S(2)}, u32[]{:S(2)}) %collective-permute-start.4) | collective-permute-done | bytes 524320 | tf_op jit(solution)/shard_map/ppermute | solution.py:184
  183.7 5.1 %collective-permute-done.5.refs_3_ = bf16[32,32,256]{2,1,0:T(8,128)(2,1)S(1)} collective-permute-done((bf16[32,32,256]{2,1,0:T(8,128)(2,1)S(1)}, bf16[32,32,256]{2,1,0:T(8,128)(2,1)S(1)}, u32[]{:S(2)}, u32[]{:S(2)}) %collective-permute-start.5) | collective-permute-done | bytes 524320 | tf_op jit(solution)/shard_map/ppermute | solution.py:181
  188.8 0.0 copy-start
  188.8 0.0 copy-start.1
  188.8 2.0 experts.1
  190.8 25.1 %all-to-all-start.1 = ((bf16[64,16,128]{2,1,0:T(8,128)(2,1)}), bf16[64,16,128]{2,1,0:T(8,128)(2,1)S(1)}, u32[]{:S(2)}, u32[]{:S(2)}) async-start(bf16[64,16,128]{2,1,0:T(8,128)(2,1)} %bitcast.6), calls=%async_computation.1 | async-start | bytes 524288 | tf_op jit(solution)/shard_map/all_to_all | solution.py:262
  215.9 0.0 copy-done
  215.9 0.0 copy-done.1
  215.9 0.4 place.1
  216.4 22.3 %all-to-all-done.1 = bf16[64,16,128]{2,1,0:T(8,128)(2,1)S(1)} async-done(((bf16[64,16,128]{2,1,0:T(8,128)(2,1)}), bf16[64,16,128]{2,1,0:T(8,128)(2,1)S(1)}, u32[]{:S(2)}, u32[]{:S(2)}) %all-to-all-start.1) | async-done | bytes 262176 | tf_op jit(solution)/shard_map/all_to_all | solution.py:262
  238.6 1.1 pick.1
Async XLA Ops:
  153.2 15.2 %collective-permute-start = (bf16[1,32,32,256]{3,2,1,0:T(8,128)(2,1)S(1)}, bf16[1,32,32,256]{3,2,1,0:T(8,128)(2,1)S(1)}, u32[]{:S(2)}, u32[]{:S(2)}) collective-permute-start(bf16[1,32,32,256]{3,2,1,0:T(8,128)(2,1)S(1)} %get-tuple-element.20.refs_0_), channel_id=1, source_target_pairs={{0,256},{256,0},{1,257},{257,1},{2,258},{258,2},{3,259},{259,3},{4... | collective-permute-start | bytes 1572872 | tf_op jit(solution)/shard_map/ppermute | solution.py:195
  157.0 18.1 %collective-permute-start.3 = (bf16[32,32,256]{2,1,0:T(8,128)(2,1)S(1)}, bf16[32,32,256]{2,1,0:T(8,128)(2,1)S(1)}, u32[]{:S(2)}, u32[]{:S(2)}) collective-permute-start(bf16[32,32,256]{2,1,0:T(8,128)(2,1)S(1)} %get-tuple-element.19.refs_0_), channel_id=1, source_target_pairs={{0,2},{1,7},{2,4},{3,1},{4,6},{5,3},{6,0},{7,5},{8,10},{9,15},{10,... | collective-permute-start | bytes 1572872 | tf_op jit(solution)/shard_map/ppermute | solution.py:181
  161.8 16.8 %collective-permute-start.1 = (bf16[1,32,32,256]{3,2,1,0:T(8,128)(2,1)S(1)}, bf16[1,32,32,256]{3,2,1,0:T(8,128)(2,1)S(1)}, u32[]{:S(2)}, u32[]{:S(2)}) collective-permute-start(bf16[1,32,32,256]{3,2,1,0:T(8,128)(2,1)S(1)} %get-tuple-element.20.refs_0_), channel_id=1, source_target_pairs={{0,1},{1,0},{2,3},{3,2},{4,5},{5,4},{6,7},{7,6},{8,9},{9,8},{10,11... | collective-permute-start | bytes 1572872 | tf_op jit(solution)/shard_map/ppermute | solution.py:236
  168.4 10.2 %collective-permute-start.2 = (bf16[1,32,32,256]{3,2,1,0:T(8,128)(2,1)S(1)}, bf16[1,32,32,256]{3,2,1,0:T(8,128)(2,1)S(1)}, u32[]{:S(2)}, u32[]{:S(2)}) collective-permute-start(bf16[1,32,32,256]{3,2,1,0:T(8,128)(2,1)S(1)} %collective-permute-done.refs_1_), channel_id=1, source_target_pairs={{0,1},{1,0},{2,3},{3,2},{4,5},{5,4},{6,7},{7,6},{8,9},{9,8},{10,11... | collective-permute-start | bytes 1572872 | tf_op jit(solution)/shard_map/ppermute | solution.py:236
  171.8 11.9 %collective-permute-start.4 = (bf16[32,32,256]{2,1,0:T(8,128)(2,1)S(1)}, bf16[32,32,256]{2,1,0:T(8,128)(2,1)S(1)}, u32[]{:S(2)}, u32[]{:S(2)}) collective-permute-start(bf16[32,32,256]{2,1,0:T(8,128)(2,1)S(1)} %get-tuple-element.19.refs_0_), channel_id=1, source_target_pairs={{0,6},{1,3},{2,0},{3,5},{4,2},{5,7},{6,4},{7,1},{8,14},{9,11},{10,... | collective-permute-start | bytes 1572872 | tf_op jit(solution)/shard_map/ppermute | solution.py:184
  175.1 13.7 %collective-permute-start.5 = (bf16[32,32,256]{2,1,0:T(8,128)(2,1)S(1)}, bf16[32,32,256]{2,1,0:T(8,128)(2,1)S(1)}, u32[]{:S(2)}, u32[]{:S(2)}) collective-permute-start(bf16[32,32,256]{2,1,0:T(8,128)(2,1)S(1)} %collective-permute-done.3.refs_1_), channel_id=1, source_target_pairs={{0,2},{1,7},{2,4},{3,1},{4,6},{5,3},{6,0},{7,5},{8,10},{9,15},{10,... | collective-permute-start | bytes 1572872 | tf_op jit(solution)/shard_map/ppermute | solution.py:181
  188.8 27.1 %copy-start = (s32[256,2]{0,1:T(2,128)S(1)}, s32[256,2]{0,1:T(2,128)}, u32[]{:S(2)}) copy-start(s32[256,2]{0,1:T(2,128)} %param.10) | copy-start | bytes 6148
  188.8 27.1 %copy-start.1 = (f32[256,2]{0,1:T(2,128)S(1)}, f32[256,2]{0,1:T(2,128)}, u32[]{:S(2)}) copy-start(f32[256,2]{0,1:T(2,128)} %param.11) | copy-start | bytes 6148
  190.8 47.8 %all-to-all-start.1 = ((bf16[64,16,128]{2,1,0:T(8,128)(2,1)}), bf16[64,16,128]{2,1,0:T(8,128)(2,1)S(1)}, u32[]{:S(2)}, u32[]{:S(2)}) async-start(bf16[64,16,128]{2,1,0:T(8,128)(2,1)} %bitcast.6), calls=%async_computation.1 | async-start | bytes 524288 | tf_op jit(solution)/shard_map/all_to_all | solution.py:262

commit v6 on v5

--- a/solution.py
+++ b/solution.py
@@ -38,7 +38,7 @@
 
 
 def pack_kernel(
-    tokens, chosen, gain, gate, up, out, tok, cho, gai, gat, upp, gains, sems, *, experts, capacity
+    tokens, chosen, gain, gate, up, out, tok, cho, gai, gat, upp, gains, mine_rows, sems, *, experts, capacity
 ):
     n, width = tok.shape
     narrow = out.shape[2]
@@ -60,14 +60,16 @@
     pick = pick.astype(F32).reshape(experts * share, n).astype(BF16)
     copies[1].wait()
     gains[...] = jnp.broadcast_to(column(gai[...]), gains.shape)
-    for c in copies[2 : 2 + PARTS]:
-        c.wait()
-    x = tok[...].astype(F32)
-    scale = lax.rsqrt(jnp.sum(x * x, axis=-1, keepdims=True) / width + 1e-06)
+    for i in range(PARTS):
+        copies[2 + i].wait()
+        x = tok[i * part : (i + 1) * part].astype(F32)
+        scale = lax.rsqrt(jnp.sum(x * x, axis=-1, keepdims=True) / width + 1e-06)
+        for c in range(CORES):
+            at = pl.multiple_of((lax.axis_index("x") * CORES + c) * narrow, narrow)
+            own = tok[i * part : (i + 1) * part, pl.ds(at, narrow)].astype(F32)
+            mine_rows[c, i * part : (i + 1) * part, :] = (own * scale).astype(BF16)
     for c in range(CORES):
-        at = pl.multiple_of((lax.axis_index("x") * CORES + c) * narrow, narrow)
-        own = (tok[:, pl.ds(at, narrow)].astype(F32) * scale).astype(BF16)
-        rows = dot(pick, own).astype(BF16).reshape(experts, share, narrow)
+        rows = dot(pick, mine_rows[c]).astype(BF16).reshape(experts, share, narrow)
         out[:, c * share : (c + 1) * share, :] = rows
     for c in copies[2 + PARTS :]:
         c.wait()
@@ -220,6 +222,7 @@
             pltpu.VMEM((experts, piece, half), F32),
             pltpu.VMEM((experts, piece, half), F32),
             pltpu.VMEM((block, half), F32),
+            pltpu.VMEM((CORES, n, narrow), BF16),
             pltpu.SemaphoreType.DMA((PARTS + 4,)),
         ],
         compiler_params=PARAMS,

time: 240 us -> 240 us (level)
  no operation moved by 1% of the time
where the time goes in v6:
time: 240 us
  blocking collectives  151 us (63%)
  starting transfers between devices  45.8 us (19%)
  waiting for transfers between devices  35.7 us (15%)
  Pallas kernels  6.82 us (3%)
    all_to_all x1, blocking collectives, on_device(): got = lax.all_to_all(sent, 'fs', split_axis=0, concat_axis=0, tiled=True)  151 us
    all_to_all x1, starting transfers between devices, on_device(): lax.all_to_all(hidden.reshape(sources * CORES, share, half), ('fs', 'core...  25.1 us
    all_to_all x1, waiting for transfers between devices, on_device(): lax.all_to_all(hidden.reshape(sources * CORES, share, half), ('fs', 'core...  22.3 us
    ppermute x2, starting transfers between devices, gather_slices(): one = lax.ppermute(one, ('x', 'core'), hop(1))  8.32 us
    ppermute x2, starting transfers between devices, on_device(): others = [lax.ppermute(w, 'core', swap) for w in weights]  5.38 us
    ppermute x2, waiting for transfers between devices, gather_slices(): one = lax.ppermute(one, ('x', 'core'), hop(1))  5.1 us
  transfers between devices with their start and end apart: 7, of which 4 were waited for; matrix products, arithmetic and copies ran while one was open for 0% of the time, Pallas kernels for 1%

profile of v6, /device:TPU:33, one launch (start us, length us, event | category | flops | bytes accessed | tf_op | source)
XLA Modules:
  0.0 239.8 jit_solution(11932946262333531376)
XLA Ops:
  0.6 2.0 pack.1
  2.7 150.5 %all_to_all.10 = bf16[32,64,256]{2,1,0:T(8,128)(2,1)S(1)} all-to-all(bf16[32,64,256]{2,1,0:T(8,128)(2,1)S(1)} %pack.1), channel_id=1, replica_groups=mesh['grp'=2,'fs'=32,'x'=4,'core'=2] {'fs'}, dimensions={0} | all-to-all | bytes 2097152 | tf_op jit(solution)/shard_map/all_to_all | solution.py:234
  153.2 0.1 fusion
  153.3 3.8 %collective-permute-start = (bf16[1,32,32,256]{3,2,1,0:T(8,128)(2,1)S(1)}, bf16[1,32,32,256]{3,2,1,0:T(8,128)(2,1)S(1)}, u32[]{:S(2)}, u32[]{:S(2)}) collective-permute-start(bf16[1,32,32,256]{3,2,1,0:T(8,128)(2,1)S(1)} %get-tuple-element.20.refs_0_), channel_id=1, source_target_pairs={{0,256},{256,0},{1,257},{257,1},{2,258},{258,2},{3,259},{259,3},{4... | collective-permute-start | bytes 1572872 | tf_op jit(solution)/shard_map/ppermute | solution.py:197
  157.1 4.8 %collective-permute-start.3 = (bf16[32,32,256]{2,1,0:T(8,128)(2,1)S(1)}, bf16[32,32,256]{2,1,0:T(8,128)(2,1)S(1)}, u32[]{:S(2)}, u32[]{:S(2)}) collective-permute-start(bf16[32,32,256]{2,1,0:T(8,128)(2,1)S(1)} %get-tuple-element.19.refs_0_), channel_id=1, source_target_pairs={{0,2},{1,7},{2,4},{3,1},{4,6},{5,3},{6,0},{7,5},{8,10},{9,15},{10,... | collective-permute-start | bytes 1572872 | tf_op jit(solution)/shard_map/ppermute | solution.py:183
  161.9 2.0 collective-permute-start.1
  163.9 4.6 %collective-permute-done.refs_1_ = bf16[1,32,32,256]{3,2,1,0:T(8,128)(2,1)S(1)} collective-permute-done((bf16[1,32,32,256]{3,2,1,0:T(8,128)(2,1)S(1)}, bf16[1,32,32,256]{3,2,1,0:T(8,128)(2,1)S(1)}, u32[]{:S(2)}, u32[]{:S(2)}) %collective-permute-start) | collective-permute-done | bytes 524320 | tf_op jit(solution)/shard_map/ppermute | solution.py:197
  168.4 3.4 %collective-permute-start.2 = (bf16[1,32,32,256]{3,2,1,0:T(8,128)(2,1)S(1)}, bf16[1,32,32,256]{3,2,1,0:T(8,128)(2,1)S(1)}, u32[]{:S(2)}, u32[]{:S(2)}) collective-permute-start(bf16[1,32,32,256]{3,2,1,0:T(8,128)(2,1)S(1)} %collective-permute-done.refs_1_), channel_id=1, source_target_pairs={{0,1},{1,0},{2,3},{3,2},{4,5},{5,4},{6,7},{7,6},{8,9},{9,8},{10,11... | collective-permute-start | bytes 1572872 | tf_op jit(solution)/shard_map/ppermute | solution.py:239
  171.9 3.3 %collective-permute-start.4 = (bf16[32,32,256]{2,1,0:T(8,128)(2,1)S(1)}, bf16[32,32,256]{2,1,0:T(8,128)(2,1)S(1)}, u32[]{:S(2)}, u32[]{:S(2)}) collective-permute-start(bf16[32,32,256]{2,1,0:T(8,128)(2,1)S(1)} %get-tuple-element.19.refs_0_), channel_id=1, source_target_pairs={{0,6},{1,3},{2,0},{3,5},{4,2},{5,7},{6,4},{7,1},{8,14},{9,11},{10,... | collective-permute-start | bytes 1572872 | tf_op jit(solution)/shard_map/ppermute | solution.py:186
  175.2 0.0 collective-permute-done.3.refs_1_
  175.2 3.5 %collective-permute-start.5 = (bf16[32,32,256]{2,1,0:T(8,128)(2,1)S(1)}, bf16[32,32,256]{2,1,0:T(8,128)(2,1)S(1)}, u32[]{:S(2)}, u32[]{:S(2)}) collective-permute-start(bf16[32,32,256]{2,1,0:T(8,128)(2,1)S(1)} %collective-permute-done.3.refs_1_), channel_id=1, source_target_pairs={{0,2},{1,7},{2,4},{3,1},{4,6},{5,3},{6,0},{7,5},{8,10},{9,15},{10,... | collective-permute-start | bytes 1572872 | tf_op jit(solution)/shard_map/ppermute | solution.py:183
  178.7 0.0 collective-permute-done.1.refs_2_
  178.7 0.0 collective-permute-done.2.refs_3_
  178.7 1.3 assemble.1
  180.0 3.8 %collective-permute-done.4.refs_2_ = bf16[32,32,256]{2,1,0:T(8,128)(2,1)S(1)} collective-permute-done((bf16[32,32,256]{2,1,0:T(8,128)(2,1)S(1)}, bf16[32,32,256]{2,1,0:T(8,128)(2,1)S(1)}, u32[]{:S(2)}, u32[]{:S(2)}) %collective-permute-start.4) | collective-permute-done | bytes 524320 | tf_op jit(solution)/shard_map/ppermute | solution.py:186
  183.8 5.1 %collective-permute-done.5.refs_3_ = bf16[32,32,256]{2,1,0:T(8,128)(2,1)S(1)} collective-permute-done((bf16[32,32,256]{2,1,0:T(8,128)(2,1)S(1)}, bf16[32,32,256]{2,1,0:T(8,128)(2,1)S(1)}, u32[]{:S(2)}, u32[]{:S(2)}) %collective-permute-start.5) | collective-permute-done | bytes 524320 | tf_op jit(solution)/shard_map/ppermute | solution.py:183
  188.9 0.0 copy-start
  188.9 0.0 copy-start.1
  188.9 2.0 experts.1
  190.9 25.1 %all-to-all-start.1 = ((bf16[64,16,128]{2,1,0:T(8,128)(2,1)}), bf16[64,16,128]{2,1,0:T(8,128)(2,1)S(1)}, u32[]{:S(2)}, u32[]{:S(2)}) async-start(bf16[64,16,128]{2,1,0:T(8,128)(2,1)} %bitcast.6), calls=%async_computation.1 | async-start | bytes 524288 | tf_op jit(solution)/shard_map/all_to_all | solution.py:265
  216.0 0.0 copy-done
  216.0 0.0 copy-done.1
  216.0 0.4 place.1
  216.4 22.3 %all-to-all-done.1 = bf16[64,16,128]{2,1,0:T(8,128)(2,1)S(1)} async-done(((bf16[64,16,128]{2,1,0:T(8,128)(2,1)}), bf16[64,16,128]{2,1,0:T(8,128)(2,1)S(1)}, u32[]{:S(2)}, u32[]{:S(2)}) %all-to-all-start.1) | async-done | bytes 262176 | tf_op jit(solution)/shard_map/all_to_all | solution.py:265
  238.7 1.1 pick.1
Async XLA Ops:
  153.3 15.2 %collective-permute-start = (bf16[1,32,32,256]{3,2,1,0:T(8,128)(2,1)S(1)}, bf16[1,32,32,256]{3,2,1,0:T(8,128)(2,1)S(1)}, u32[]{:S(2)}, u32[]{:S(2)}) collective-permute-start(bf16[1,32,32,256]{3,2,1,0:T(8,128)(2,1)S(1)} %get-tuple-element.20.refs_0_), channel_id=1, source_target_pairs={{0,256},{256,0},{1,257},{257,1},{2,258},{258,2},{3,259},{259,3},{4... | collective-permute-start | bytes 1572872 | tf_op jit(solution)/shard_map/ppermute | solution.py:197
  157.1 18.1 %collective-permute-start.3 = (bf16[32,32,256]{2,1,0:T(8,128)(2,1)S(1)}, bf16[32,32,256]{2,1,0:T(8,128)(2,1)S(1)}, u32[]{:S(2)}, u32[]{:S(2)}) collective-permute-start(bf16[32,32,256]{2,1,0:T(8,128)(2,1)S(1)} %get-tuple-element.19.refs_0_), channel_id=1, source_target_pairs={{0,2},{1,7},{2,4},{3,1},{4,6},{5,3},{6,0},{7,5},{8,10},{9,15},{10,... | collective-permute-start | bytes 1572872 | tf_op jit(solution)/shard_map/ppermute | solution.py:183
  161.9 16.8 %collective-permute-start.1 = (bf16[1,32,32,256]{3,2,1,0:T(8,128)(2,1)S(1)}, bf16[1,32,32,256]{3,2,1,0:T(8,128)(2,1)S(1)}, u32[]{:S(2)}, u32[]{:S(2)}) collective-permute-start(bf16[1,32,32,256]{3,2,1,0:T(8,128)(2,1)S(1)} %get-tuple-element.20.refs_0_), channel_id=1, source_target_pairs={{0,1},{1,0},{2,3},{3,2},{4,5},{5,4},{6,7},{7,6},{8,9},{9,8},{10,11... | collective-permute-start | bytes 1572872 | tf_op jit(solution)/shard_map/ppermute | solution.py:239
  168.4 10.2 %collective-permute-start.2 = (bf16[1,32,32,256]{3,2,1,0:T(8,128)(2,1)S(1)}, bf16[1,32,32,256]{3,2,1,0:T(8,128)(2,1)S(1)}, u32[]{:S(2)}, u32[]{:S(2)}) collective-permute-start(bf16[1,32,32,256]{3,2,1,0:T(8,128)(2,1)S(1)} %collective-permute-done.refs_1_), channel_id=1, source_target_pairs={{0,1},{1,0},{2,3},{3,2},{4,5},{5,4},{6,7},{7,6},{8,9},{9,8},{10,11... | collective-permute-start | bytes 1572872 | tf_op jit(solution)/shard_map/ppermute | solution.py:239
  171.9 11.9 %collective-permute-start.4 = (bf16[32,32,256]{2,1,0:T(8,128)(2,1)S(1)}, bf16[32,32,256]{2,1,0:T(8,128)(2,1)S(1)}, u32[]{:S(2)}, u32[]{:S(2)}) collective-permute-start(bf16[32,32,256]{2,1,0:T(8,128)(2,1)S(1)} %get-tuple-element.19.refs_0_), channel_id=1, source_target_pairs={{0,6},{1,3},{2,0},{3,5},{4,2},{5,7},{6,4},{7,1},{8,14},{9,11},{10,... | collective-permute-start | bytes 1572872 | tf_op jit(solution)/shard_map/ppermute | solution.py:186
  175.2 13.7 %collective-permute-start.5 = (bf16[32,32,256]{2,1,0:T(8,128)(2,1)S(1)}, bf16[32,32,256]{2,1,0:T(8,128)(2,1)S(1)}, u32[]{:S(2)}, u32[]{:S(2)}) collective-permute-start(bf16[32,32,256]{2,1,0:T(8,128)(2,1)S(1)} %collective-permute-done.3.refs_1_), channel_id=1, source_target_pairs={{0,2},{1,7},{2,4},{3,1},{4,6},{5,3},{6,0},{7,5},{8,10},{9,15},{10,... | collective-permute-start | bytes 1572872 | tf_op jit(solution)/shard_map/ppermute | solution.py:183
  188.9 27.1 %copy-start = (s32[256,2]{0,1:T(2,128)S(1)}, s32[256,2]{0,1:T(2,128)}, u32[]{:S(2)}) copy-start(s32[256,2]{0,1:T(2,128)} %param.10) | copy-start | bytes 6148
  188.9 27.1 %copy-start.1 = (f32[256,2]{0,1:T(2,128)S(1)}, f32[256,2]{0,1:T(2,128)}, u32[]{:S(2)}) copy-start(f32[256,2]{0,1:T(2,128)} %param.11) | copy-start | bytes 6148
  190.9 47.8 %all-to-all-start.1 = ((bf16[64,16,128]{2,1,0:T(8,128)(2,1)}), bf16[64,16,128]{2,1,0:T(8,128)(2,1)S(1)}, u32[]{:S(2)}, u32[]{:S(2)}) async-start(bf16[64,16,128]{2,1,0:T(8,128)(2,1)} %bitcast.6), calls=%async_computation.1 | async-start | bytes 524288 | tf_op jit(solution)/shard_map/all_to_all | solution.py:265
